TPU v7x, 512 devices: a whole 4x8x8 slice. The times are simulated.
512 devices in a mesh: sp: 64 (over z, y), tp: 8 (over x, core).
Axes of the slice: x: 4, y: 8, z: 8, core: 2. Of those that a mesh axis runs over, the one named last changes fastest.
Arguments:
- skip_stream_entering: bfloat16 [4096, 2048], P('sp'), may hold values from -6 to 6
- reading_vectors: bfloat16 [4096, 1024], P('sp', 'tp'), may hold values from -6 to 6
- blender_lookup_labels: bfloat16 [4096, 1024], P('sp', 'tp'), may hold values from -6 to 6
- blender_payloads: bfloat16 [4096, 1024], P('sp', 'tp'), may hold values from -6 to 6
- blender_result_valve: bfloat16 [4096, 1024], P('sp', 'tp'), may hold values from -6 to 6
- fading_logits: bfloat16 [2, 4096, 1024], P(None, 'sp', 'tp'), as said below
- amend_speed_logits: bfloat16 [2, 4096, 1024], P(None, 'sp', 'tp'), as said below
- extra_log_fades: float32 [2, 16, 4096], P(None, 'tp', 'sp'), may hold values from -3 to 0
- present_reward_factors: float32 [1024], P('tp'), may hold values from -1.2 to 1.2
- attender_scaling_vector: float32 [1024], P('tp'), may hold values from 0.1 to 1.9
- blender_result_projector: bfloat16 [1024, 2048], P('tp'), may hold values from -0.1875 to 0.1875
- blender_scaling_vector: float32 [2048], replicated, may hold values from 0.1 to 1.9
- perceptron_valve_factors: bfloat16 [2048, 5632], P('sp', 'tp'), may hold values from -0.125 to 0.125
- perceptron_widen_factors: bfloat16 [2048, 5632], P('sp', 'tp'), may hold values from -0.125 to 0.125
- perceptron_shrink_factors: bfloat16 [5632, 2048], P('tp', 'sp'), may hold values from -0.078125 to 0.078125
- closing_scaling_vector: float32 [2048], replicated, may hold values from 0.1 to 1.9
Outputs:
- result: bfloat16 [4096, 2048], P(('sp', 'tp'))
Inputs may be any that keep to these rules, and one draw needn't show every extreme that they name: `fading_logits`: decay pre-activations. `amend_speed_logits`: correction-rate pre-activations.
All inputs are finite; a program needn't handle non-finite values.
Results may differ from a plain program's by a relative error of at most 0.02.
Values may be sent and summed in bfloat16 or wider, within the bound.
A program may use at most 64 MiB of HBM per device.

v0:
```python
import jax
import jax.numpy as jnp
from jax import lax
from jax.sharding import Mesh
from jax.sharding import PartitionSpec as P

SP = ("sp_0", "sp_1")
SP_TP = ("sp_0", "sp_1", "tp")


RESIDUAL_SCALE = 2.0**0.25
NORM_EPS = 1e-05
GROUP_EPS = 0.00064
KEY_EPS = 1e-06


def turned_gather(arrays, axis, dims):
    turned = [jnp.moveaxis(a, dim, 0) for a, dim in zip(arrays, dims)]
    widths = [t[0].size for t in turned]
    both = jnp.concatenate([t.reshape(-1, w) for t, w in zip(turned, widths)], axis=1)
    whole = lax.all_gather(both, axis, axis=0, tiled=True)
    blocks = jnp.split(whole, [sum(widths[:k]) for k in range(1, len(widths))], axis=1)
    return tuple(
        (
            jnp.moveaxis(b.reshape(-1, *t.shape[1:]), 0, dim)
            for b, t, dim in zip(blocks, turned, dims)
        )
    )


def nothing_yet(value, identity):
    return jax.tree.map(
        lambda part, zero: jnp.zeros_like(part) + jnp.asarray(zero, part.dtype), value, identity
    )


def collected_together(value, axis):
    leaves = jax.tree.leaves(value)
    order = sorted(range(len(leaves)), key=lambda k: -leaves[k].size)
    width = (1, *leaves[order[0]].shape)[-1]
    lines = [
        jnp.pad(leaves[k].reshape(-1), (0, -leaves[k].size % width)).reshape(-1, width)
        for k in order
    ]
    both, at, found = (lax.all_gather(jnp.concatenate(lines), axis), 0, {})
    for k, line in zip(order, lines):
        share = both[:, at : at + len(line)].reshape(len(both), -1)
        found[k] = share[:, : leaves[k].size].reshape(-1, *leaves[k].shape)
        at += len(line)
    numbers = iter(range(len(leaves)))
    return jax.tree.map(lambda _: found[next(numbers)], value)


def carried_in(value, axes, combine, identity, reverse):
    before = start = nothing_yet(value, identity)
    total = value
    for axis in reversed(axes):
        length, position = (lax.axis_size(axis), lax.axis_index(axis))
        pieces = collected_together(
            jax.tree.map(lambda part, kind: part.astype(kind), total, (jnp.bfloat16, jnp.bfloat16)),
            axis,
        )
        inside, total = (start, start)
        for k in reversed(range(length)) if reverse else range(length):
            passed = k > position if reverse else k < position
            total = combine(
                total, jax.tree.map(lambda part, own: part[k].astype(own.dtype), pieces, value)
            )
            inside = jax.tree.map(lambda new, old: jnp.where(passed, new, old), total, inside)
        before = combine(inside, before)
    return before


def cut_along(value, dim, length):
    before, after = (value.shape[:dim], value.shape[dim + 1 :])
    return jnp.moveaxis(value.reshape(*before, length, -1, *after), dim, 0)


def sent_and_summed(value, axis, dim):
    length = lax.axis_size(axis)
    blocks = lax.all_to_all(cut_along(value, dim, length), axis, 0, 0, tiled=True)
    return jnp.sum(blocks.astype(jnp.float32), axis=0)


def joined_along(blocks, dim):
    dims = list(blocks.shape[1:])
    dims[dim] *= blocks.shape[0]
    return jnp.moveaxis(blocks, 0, dim).reshape(dims)


def sent_to_all(value, axis):
    copies = jnp.broadcast_to(value, (lax.axis_size(axis), *value.shape))
    return lax.all_to_all(copies, axis, split_axis=0, concat_axis=0, tiled=True)


def gathered_copies(value, axis, dim):
    return joined_along(sent_to_all(value, axis), dim)


def layer_norm(summand, gain_vec):
    center = jnp.mean(summand, -1, keepdims=True)
    spread = jnp.mean(jnp.square(summand - center), -1, keepdims=True)
    return (summand - center) * lax.rsqrt(spread + NORM_EPS) * gain_vec


def chain_blocks(earlier, later):
    return (
        jnp.einsum("hij,hjk->hik", earlier[0], later[0]),
        jnp.einsum("hij,hjk->hik", earlier[1], later[0]) + later[1],
    )


def advance(joined, inputs):
    query_vec, decay_vec, write_key, padded_value, erase_vec, refill_vec = inputs
    erased = jnp.einsum("hji,hj->hi", joined, erase_vec)
    joined = (
        joined * decay_vec[:, :, None]
        + refill_vec[:, :, None] * erased[:, None, :]
        + write_key[:, :, None] * padded_value[:, None, :]
    )
    return (joined, jnp.einsum("hji,hj->hi", joined, query_vec))


def shards(
    skip_stream_entering,
    reading_vectors,
    blender_lookup_labels,
    blender_payloads,
    blender_result_valve,
    fading_logits,
    amend_speed_logits,
    extra_log_fades,
    present_reward_factors,
    attender_scaling_vector,
    blender_result_projector,
    blender_scaling_vector,
    perceptron_valve_factors,
    perceptron_widen_factors,
    perceptron_shrink_factors,
    closing_scaling_vector,
):
    whole_gate, whole_up, whole_down = turned_gather(
        (perceptron_valve_factors, perceptron_widen_factors, perceptron_shrink_factors),
        SP,
        (0, 0, 1),
    )
    tok_rows = reading_vectors.shape[0]
    local_attender_number = extra_log_fades.shape[1]
    head_size = reading_vectors.shape[1] // local_attender_number
    row_share = tok_rows // lax.axis_size("tp")
    row_start = lax.axis_index("tp") * row_share

    def split_attenders(tensor):
        return tensor.reshape(tensor.shape[:-1] + (local_attender_number, head_size))

    def both_ways(forward_part, backward_part):
        return jnp.concatenate([forward_part, jnp.flip(backward_part, 0)], axis=1)

    entire_asking_lines = split_attenders(reading_vectors.astype(jnp.float32))
    key_rows = split_attenders(blender_lookup_labels.astype(jnp.float32))
    payload_line_slab = split_attenders(blender_payloads.astype(jnp.float32))
    key_square = jnp.sum(key_rows * key_rows, -1, keepdims=True)
    unit_keys = key_rows * lax.rsqrt(key_square + KEY_EPS)
    fading_log_amount = (
        split_attenders(-jnp.exp(-jax.nn.softplus(-fading_logits.astype(jnp.float32)) - 0.5))
        + jnp.swapaxes(extra_log_fades, 1, 2)[..., None]
    )
    decays = jnp.exp(fading_log_amount)
    icl_rates = split_attenders(jax.nn.sigmoid(amend_speed_logits.astype(jnp.float32)))
    stored_label_lines = key_rows[None] * icl_rates
    refills = unit_keys[None] * icl_rates
    padded_payload = jnp.concatenate(
        [payload_line_slab, jnp.zeros_like(payload_line_slab)], axis=-1
    )
    sequence_in = (
        both_ways(entire_asking_lines, entire_asking_lines),
        both_ways(decays[0], decays[1]),
        both_ways(stored_label_lines[0], stored_label_lines[1]),
        both_ways(padded_payload, padded_payload),
        both_ways(-unit_keys, -unit_keys),
        both_ways(refills[0], refills[1]),
    )
    identity = jnp.broadcast_to(
        jnp.eye(head_size, dtype=jnp.float32), (2 * local_attender_number, head_size, head_size)
    )
    start_joined = jnp.concatenate([jnp.zeros_like(identity), identity], axis=-1)
    joined_end, readings = lax.scan(advance, start_joined, sequence_in, unroll=16)
    state_end = jnp.swapaxes(joined_end[..., :head_size], 1, 2)
    prod_end = jnp.swapaxes(joined_end[..., head_size:], 1, 2)
    local_out = readings[..., :head_size]
    carried_dir = readings[..., head_size:]
    neutral = (identity[:local_attender_number], jnp.zeros_like(identity[:local_attender_number]))
    enter_fwd = carried_in(
        (prod_end[:local_attender_number], state_end[:local_attender_number]),
        SP,
        chain_blocks,
        neutral,
        False,
    )[1]
    enter_bwd = carried_in(
        (prod_end[local_attender_number:], state_end[local_attender_number:]),
        SP,
        chain_blocks,
        neutral,
        True,
    )[1]
    entering = jnp.concatenate([enter_fwd, enter_bwd], axis=0)
    complete = local_out + jnp.einsum("hij,thj->thi", entering, carried_dir)
    summed = complete[:, :local_attender_number] + jnp.flip(complete[:, local_attender_number:], 0)
    center = jnp.mean(summed, -1, keepdims=True)
    spread = jnp.mean(jnp.square(summed - center), -1, keepdims=True)
    rescaled_lines = (
        (summed - center) * lax.rsqrt(spread + GROUP_EPS) * split_attenders(attender_scaling_vector)
    )
    present_reward_summand = (
        jnp.sum(
            entire_asking_lines
            * (stored_label_lines[0] + stored_label_lines[1])
            * split_attenders(present_reward_factors),
            -1,
            keepdims=True,
        )
        * payload_line_slab
    )
    merged_attender_lines = (
        (rescaled_lines + present_reward_summand)
        * split_attenders(blender_result_valve.astype(jnp.float32))
    ).reshape(tok_rows, -1)
    merged_attender_lines = merged_attender_lines.astype(jnp.bfloat16)
    picked = merged_attender_lines
    mixsum = sent_and_summed(
        jnp.dot(picked, blender_result_projector, preferred_element_type=jnp.float32).astype(
            jnp.bfloat16
        ),
        "tp",
        0,
    )
    residual = lax.dynamic_slice_in_dim(skip_stream_entering, row_start, row_share, 0).astype(
        jnp.float32
    )
    middle = layer_norm(RESIDUAL_SCALE * residual + mixsum, blender_scaling_vector).astype(
        jnp.bfloat16
    )
    all_middle = gathered_copies(middle, "tp", 0)
    gate_pre = jnp.dot(all_middle, whole_gate, preferred_element_type=jnp.float32)
    up_pre = jnp.dot(all_middle, whole_up, preferred_element_type=jnp.float32)
    inner_act = (jax.nn.silu(gate_pre) * up_pre).astype(jnp.bfloat16)
    picked = inner_act
    downsum = sent_and_summed(
        jnp.dot(picked, whole_down, preferred_element_type=jnp.float32).astype(jnp.bfloat16),
        "tp",
        0,
    )
    return layer_norm(
        RESIDUAL_SCALE * middle.astype(jnp.float32) + downsum, closing_scaling_vector
    ).astype(jnp.bfloat16)


def solution(mesh):
    finer = Mesh(mesh.devices.reshape(8, 8, mesh.shape["tp"]), ("sp_0", "sp_1", "tp"))
    placed = (
        P(SP, None),
        P(SP, "tp"),
        P(SP, "tp"),
        P(SP, "tp"),
        P(SP, "tp"),
        P(None, SP, "tp"),
        P(None, SP, "tp"),
        P(None, "tp", SP),
        P("tp"),
        P("tp"),
        P("tp", None),
        P(),
        P(SP, "tp"),
        P(SP, "tp"),
        P("tp", SP),
        P(),
    )
    return jax.shard_map(
        shards, mesh=finer, in_specs=placed, out_specs=P(SP_TP, None), check_vma=False
    )
```

profile of v0, /device:TPU:1, one launch (start us, length us, event | category | flops | bytes accessed | tf_op | source)
XLA Modules:
  0.0 250.0 jit_solution(18129958228404149281)
XLA Ops:
  6.5 1.7 concatenate.86
  8.3 0.8 reshape.622
  9.1 0.8 concatenate.78
  12.3 0.8 fusion.136
  14.3 0.8 reshape.639
  15.7 61.7 %while.12 = (s32[]{:T(128)}, f32[4,64,128]{2,1,0:T(8,128)S(1)}, f32[4,16,4,128]{3,1,0,2:T(8,128)S(1)}, f32[4,16,4,64]{3,2,1,0:T(4,128)S(1)}, f32[4,16,4,64]{3,2,...) while((s32[]{:T(128)}, f32[4,64,128]{2,1,0:T(8,128)S(1)}, ...), condition=%wide.region_2.3_spmd, body=%wide.region_1.2_spmd.sunk | while | flops 16515089 | bytes 6333085 | solution.py:187
  19.2 0.9 multiply_add_fusion.103
  21.4 1.3 multiply_add_fusion.104
  29.2 1.8 multiply_add_fusion.105
  34.7 0.9 multiply_add_fusion.103
  36.9 1.3 multiply_add_fusion.104
  44.7 1.8 multiply_add_fusion.105
  50.1 0.9 multiply_add_fusion.103
  52.3 1.3 multiply_add_fusion.104
  60.1 1.8 multiply_add_fusion.105
  65.5 0.9 multiply_add_fusion.103
  67.8 1.3 multiply_add_fusion.104
  75.5 1.8 multiply_add_fusion.105
  77.9 25.0 %all-gather = bf16[2048,64]{0,1:T(8,128)(2,1)S(1)} all-gather(bf16[256,64]{0,1:T(8,128)(2,1)S(1)} %pad_maximum_fusion.8), channel_id=2, replica_groups=mesh['sp_0'=8,'sp_1'=8,'tp'=8] {'sp_1'}, dimensions={0}, use_global_device_ids=true | all-gather | bytes 294912 | tf_op jit(solution)/shard_map/all_gather | solution.py:45
  103.5 22.1 %all-gather.2 = bf16[2048,64]{0,1:T(8,128)(2,1)S(1)} all-gather(bf16[256,64]{0,1:T(8,128)(2,1)S(1)} %pad_maximum_fusion.9), channel_id=4, replica_groups=mesh['sp_0'=8,'sp_1'=8,'tp'=8] {'sp_1'}, dimensions={0}, use_global_device_ids=true | all-gather | bytes 294912 | tf_op jit(solution)/shard_map/all_gather | solution.py:45
  130.3 24.4 %all-gather.1 = bf16[2048,64]{1,0:T(8,128)(2,1)S(1)} all-gather(bf16[256,64]{1,0:T(8,128)(2,1)S(1)} %pad_maximum_fusion.6), channel_id=3, replica_groups=mesh['sp_0'=8,'sp_1'=8,'tp'=8] {'sp_0'}, dimensions={0}, use_global_device_ids=true | all-gather | bytes 294912 | tf_op jit(solution)/shard_map/all_gather | solution.py:45
  154.7 19.6 %all-gather.3 = bf16[2048,64]{1,0:T(8,128)(2,1)S(1)} all-gather(bf16[256,64]{1,0:T(8,128)(2,1)S(1)} %pad_maximum_fusion.7), channel_id=5, replica_groups=mesh['sp_0'=8,'sp_1'=8,'tp'=8] {'sp_0'}, dimensions={0}, use_global_device_ids=true | all-gather | bytes 294912 | tf_op jit(solution)/shard_map/all_gather | solution.py:45
  178.7 0.9 fusion.97
  179.7 25.6 %all-to-all-start = ((bf16[8,8,2048]{2,1,0:T(8,128)(2,1)}), bf16[8,8,2048]{2,1,0:T(8,128)(2,1)S(1)}, u32[]{:S(2)}, u32[]{:S(2)}) async-start(bf16[8,8,2048]{2,1,0:T(8,128)(2,1)} %fusion.97), calls=%async_computation | async-start | bytes 524288 | tf_op jit(solution)/shard_map/all_to_all | solution.py:81
  205.3 6.5 %all-to-all-done = bf16[8,8,2048]{2,1,0:T(8,128)(2,1)S(1)} async-done(((bf16[8,8,2048]{2,1,0:T(8,128)(2,1)}), bf16[8,8,2048]{2,1,0:T(8,128)(2,1)S(1)}, u32[]{:S(2)}, u32[]{:S(2)}) %all-to-all-start) | async-done | bytes 262176 | tf_op jit(solution)/shard_map/all_to_all | solution.py:81
  211.8 0.9 fusion.256
  212.7 1.0 multiply_reduce_fusion.1
  213.7 0.8 multiply_convert_fusion.1
  214.6 9.9 %all_to_all.15 = bf16[8,8,2048]{2,1,0:T(8,128)(2,1)S(1)} all-to-all(bf16[8,8,2048]{2,1,0:T(8,128)(2,1)S(1)} %broadcast_in_dim.79), channel_id=1, replica_groups=mesh['sp_0'=8,'sp_1'=8,'tp'=8] {'tp'}, dimensions={0} | all-to-all | bytes 524288 | tf_op jit(solution)/shard_map/all_to_all | solution.py:93
  224.5 2.5 %fusion.92 = f32[64,704]{1,0:T(8,128)S(1)} fusion(bf16[2048,2112]{1,0:T(8,128)(2,1)} %all-gather.6.cloned.1.call-done, bf16[8,8,2048]{2,1,0:T(8,128)(2,1)S(1)} %all_to_all.15), kind=kOutput, calls=%fused_computation.221 | convolution fusion | flops 184549376 | bytes 3588096 | tf_op jit(solution)/shard_map/dot_general | solution.py:245
  227.0 5.2 %fusion.98 = bf16[8,8,2048]{2,1,0:T(8,128)(2,1)S(1)} fusion(bf16[2048,2112]{1,0:T(8,128)(2,1)} %all-gather.6.cloned.1.call-done, bf16[8,8,2048]{2,1,0:T(8,128)(2,1)S(1)} %all_to_all.15, f32[64,704]{1,0:T(8,128)S(1)} %fusion.92), kind=kOutput, calls=%fused_computation.226 | convolution fusion | flops 369500160 | bytes 6995968 | tf_op jit(solution)/shard_map/dot_general | solution.py:250
  232.2 9.9 %all_to_all.16 = bf16[8,8,2048]{2,1,0:T(8,128)(2,1)S(1)} all-to-all(bf16[8,8,2048]{2,1,0:T(8,128)(2,1)S(1)} %fusion.98), channel_id=1, replica_groups=mesh['sp_0'=8,'sp_1'=8,'tp'=8] {'tp'}, dimensions={0} | all-to-all | bytes 524288 | tf_op jit(solution)/shard_map/all_to_all | solution.py:81
  (357 shorter events, 60.5 us)
Async XLA Ops:
  6.5 172.2 %copy-start = (bf16[128,2048]{1,0:T(8,128)(2,1)S(1)}, bf16[128,2048]{1,0:T(8,128)(2,1)}, u32[]{:S(2)}) copy-start(bf16[128,2048]{1,0:T(8,128)(2,1)} %param.28) | copy-start | bytes 1572868
  6.5 217.9 %all-gather.6.cloned.1.call-start = ((), (), s32[]{:S(2)}) async-start(), calls=%async_computation.3 | async-start | bytes 9052160 | tf_op jit(solution)/shard_map/all_gather | solution.py:21
  77.5 100.2 %copy-start.4 = (f32[128]{0:T(128)S(1)}, f32[128]{0:T(128)}, u32[]{:S(2)}) copy-start(f32[128]{0:T(128)} %param.26) | copy-start | bytes 1540
  77.6 100.4 %copy-start.1 = (bf16[64,128]{1,0:T(8,128)(2,1)S(1)}, bf16[64,128]{1,0:T(8,128)(2,1)}, u32[]{:S(2)}) copy-start(bf16[64,128]{1,0:T(8,128)(2,1)} %param.22) | copy-start | bytes 49156
  77.6 100.5 %copy-start.5 = (f32[128]{0:T(128)S(1)}, f32[128]{0:T(128)}, u32[]{:S(2)}) copy-start(f32[128]{0:T(128)} %param.27) | copy-start | bytes 1540
  125.6 88.1 %copy-start.2 = (f32[2048]{0:T(1024)S(1)}, f32[2048]{0:T(1024)}, u32[]{:S(2)}) copy-start(f32[2048]{0:T(1024)} %param.29) | copy-start | bytes 24580
  177.4 65.1 %copy-start.3 = (f32[2048]{0:T(1024)S(1)}, f32[2048]{0:T(1024)}, u32[]{:S(2)}) copy-start(f32[2048]{0:T(1024)} %param.33) | copy-start | bytes 24580
  179.7 32.1 %all-to-all-start = ((bf16[8,8,2048]{2,1,0:T(8,128)(2,1)}), bf16[8,8,2048]{2,1,0:T(8,128)(2,1)S(1)}, u32[]{:S(2)}, u32[]{:S(2)}) async-start(bf16[8,8,2048]{2,1,0:T(8,128)(2,1)} %fusion.97), calls=%async_computation | async-start | bytes 524288 | tf_op jit(solution)/shard_map/all_to_all | solution.py:81
Sparse Core Ops, SparseCore 0:
  10.3 110.1 all-gather.5
where the time goes:
time: 251 us; the launch traced here: 250 us
  blocking collectives  111 us (44%)
  matrix products  57.5 us (23%)
  starting transfers between devices  25.6 us (10%)
  other arithmetic  24.8 us (10%)
  between operations  14.1 us (6%)
  local copies, waits for them, and re-layouts  10.3 us (4%)
  waiting for transfers between devices  6.49 us (3%)
    all_gather x4, blocking collectives, collected_together(): both, at, found = (lax.all_gather(jnp.concatenate(lines), axis), 0, {})  91.1 us
    all_to_all x1, starting transfers between devices, sent_and_summed(): lax.all_to_all(cut_along(value, dim, length), axis, 0, 0, tiled=True)  25.6 us
    dot_general x64, matrix products, advance(): return (joined, jnp.einsum('hji,hj->hi', joined, query_vec))  20.8 us
    dot_general x64, matrix products, advance(): erased = jnp.einsum('hji,hj->hi', joined, erase_vec)  20.7 us
    add x16, other arithmetic, advance(): joined * decay_vec[:, :, None] + refill_vec[:, :, None] * erased[:, None, :]  17.8 us
    all_to_all x1, blocking collectives, sent_to_all(): return lax.all_to_all(copies, axis, split_axis=0, concat_axis=0, tiled=True)  9.91 us
    all_to_all x1, blocking collectives, sent_and_summed(): lax.all_to_all(cut_along(value, dim, length), axis, 0, 0, tiled=True)  9.91 us
    all_to_all x1, waiting for transfers between devices, sent_and_summed(): lax.all_to_all(cut_along(value, dim, length), axis, 0, 0, tiled=True)  6.47 us
  transfers between devices with their start and end apart: 2, of which 1 were waited for; matrix products, arithmetic and copies ran while one was open for 33% of the time, Pallas kernels for 0%

commit v1 on v0

v1 whole, which is shorter than its diff:
```python
import jax
import jax.numpy as jnp
from jax import lax
from jax.experimental import pallas as pl
from jax.experimental.pallas import tpu as pltpu
from jax.sharding import Mesh
from jax.sharding import PartitionSpec as P

SP = ("sp_0", "sp_1")
SP_TP = ("sp_0", "sp_1", "tp")
MESH = pl.DeviceIdType.MESH
F32 = jnp.float32
BF16 = jnp.bfloat16
HIGHEST = lax.Precision.HIGHEST

RESIDUAL_SCALE = 2.0**0.25
NORM_EPS = 1e-05
GROUP_EPS = 0.00064
KEY_EPS = 1e-06
HALF_EXP = 0.6065306597126334

TOK = 64
LANES = 128
WA_COLS = 1152
WB_COLS = 1024


def dot(a, b, ca=1, cb=0):
    return lax.dot_general(
        a, b, (((ca,), (cb,)), ((), ())), precision=HIGHEST, preferred_element_type=F32
    )


def bdot(a, b, ca=1, cb=0):
    return lax.dot_general(
        a.astype(BF16), b.astype(BF16), (((ca,), (cb,)), ((), ())), preferred_element_type=F32
    )


def iota(shape, dim):
    return lax.broadcasted_iota(jnp.int32, shape, dim)


def expand(x):
    lane = iota(x.shape, 1)
    zero = jnp.zeros_like(x)
    return jnp.concatenate([jnp.where(lane < 64, x, zero), jnp.where(lane >= 64, x, zero)], 0)


def fold(z):
    half = z.shape[0] // 2
    return z[:half] + z[half:]


def head_ones():
    return jnp.where((iota((128, 128), 0) < 64) == (iota((128, 128), 1) < 64), 1.0, 0.0).astype(F32)


def local_mixer(q, key, val, inv, fade, amend, extra, d):
    row, col = iota((64, 64), 0), iota((64, 64), 1)
    k = key * jax.nn.sigmoid(amend)
    logw = extra - jax.nn.sigmoid(fade) * HALF_EXP
    tri = jnp.where(col <= row if d == 0 else col >= row, 1.0, 0.0).astype(F32)
    c = dot(tri, logw)
    cx = c - logw
    end = c[63:64] if d == 0 else c[0:1]
    un = key * inv * inv
    erase_rows, read_rows = [], []
    for i in range(4):
        lo = 16 * i
        ref = cx[lo : lo + 1] if d == 0 else cx[lo + 15 : lo + 16]
        kk = k * jnp.exp(jnp.minimum(ref - c, 60.0))
        lu = un[lo : lo + 16] * jnp.exp(cx[lo : lo + 16] - ref)
        lq = q[lo : lo + 16] * jnp.exp(c[lo : lo + 16] - ref)
        res = bdot(jnp.concatenate([lu, lq], 0), expand(kk), 1, 1)
        erase_rows.append(res[:16])
        read_rows.append(res[16:])
    m_all = jnp.concatenate(erase_rows, 0)
    g_all = jnp.concatenate(read_rows, 0)
    rt, ct = iota((64, 128), 0), iota((64, 128), 1) & 63
    m_all = expand(jnp.where(ct < rt if d == 0 else ct > rt, m_all, 0.0))
    g_all = jnp.where(ct <= rt if d == 0 else ct >= rt, g_all, 0.0)
    r, cc = iota((128, 128), 0), iota((128, 128), 1)
    eye = jnp.where(r == cc, 1.0, 0.0).astype(F32)
    inverse = eye - jnp.where((r >> 1) == (cc >> 1), m_all, 0.0)
    for b in range(1, 6):
        off = jnp.where(((r >> (b + 1)) == (cc >> (b + 1))) & ((r >> b) != (cc >> b)), m_all, 0.0)
        inverse = inverse - dot(dot(inverse, off), inverse)
    ut = un * jnp.exp(cx)
    vw = dot(inverse, jnp.concatenate([expand(val), expand(ut)], 1))
    kend = expand(k * jnp.exp(end - c))
    z = bdot(vw, kend, 0, 0)
    written = fold(z[:128])
    passed = jnp.where(rt == ct, jnp.exp(end), 0.0) - fold(z[128:])
    return k, passed, written, g_all, vw, q * jnp.exp(c)


def body(
    skip_ref, q_ref, key_ref, val_ref, valve_ref, fade_ref, amend_ref, extra_ref, bonus_ref,
    again_ref, proj_ref, mgain_ref, wa_ref, wb_ref, cgain_ref, out_ref,
    wa, wb, pb, c1s, c1r, c2s, c2r, c3s, c3r, mb, rs, rr, midf, midb, gu,
    a1s, a1r, b1s, b1r, a2s, a2r, b2s, b2r, p1s, p1r, p2s, p2r, p3s, p3r,
    x1s, x1r, x2s, x2r, x3s, x3r, ms, mr, ds, dr,
):
    z, y, tp = lax.axis_index("sp_0"), lax.axis_index("sp_1"), lax.axis_index("tp")
    xc, core = tp // 2, tp % 2
    partner = tp + 1 - 2 * core

    def up(at, j, n=8):
        return lax.rem(at + j, n)

    def down(at, j, n=8):
        return lax.rem(at + n - j, n)

    def copy(src, dst, send, recv, axis, at):
        return pltpu.make_async_remote_copy(
            src_ref=src, dst_ref=dst, send_sem=send, recv_sem=recv,
            device_id={axis: at}, device_id_type=MESH,
        )

    barrier = pltpu.get_barrier_semaphore()
    for axis, at in (("sp_0", z), ("sp_1", y), ("tp", tp)):
        for j in range(1, 8):
            pl.semaphore_signal(barrier, inc=1, device_id={axis: up(at, j)}, device_id_type=MESH)
    pl.semaphore_wait(barrier, 21)

    sent = []

    def go(c):
        c.start()
        sent.append(c)

    order = (1, 7, 2, 6, 3, 5, 4)
    for j in order:
        go(copy(wa_ref, wa.at[z, y], a1s.at[j - 1], a1r.at[j - 1], "sp_1", up(y, j)))
        go(copy(wb_ref, wb.at[z, y], b1s.at[j - 1], b1r.at[j - 1], "sp_0", up(z, j)))
    for j in (1, 3, 2):
        go(copy(proj_ref, pb.at[tp], p1s.at[j - 1], p1r.at[j - 1], "tp", 2 * up(xc, j, 4) + core))
    go(copy(proj_ref, pb.at[tp], p2s.at[0], p2r.at[0], "tp", partner))
    wa[z, y] = wa_ref[...]
    wb[z, y] = wb_ref[...]
    pb[tp] = proj_ref[...]

    q, key, val = q_ref[...].astype(F32), key_ref[...].astype(F32), val_ref[...].astype(F32)
    ones = head_ones()
    inv = lax.rsqrt(dot(key * key, ones) + KEY_EPS)
    sides = []
    for d in range(2):
        k, passed, written, g_all, vw, qc = local_mixer(
            q, key, val, inv, fade_ref[d].astype(F32), amend_ref[d].astype(F32), extra_ref[d], d
        )
        passed, written = passed.astype(BF16), written.astype(BF16)
        for part in range(4):
            c1s[4 * d + part] = jnp.concatenate([passed, written[16 * part : 16 * part + 16]], 0)
        sides.append((k, g_all, vw, qc))
    for j in order:
        w = up(y, j)
        go(copy(c1s.at[w], c1r.at[y], x1s.at[j - 1], x1r.at[j - 1], "sp_1", w))
    c1r[y] = c1s[y]

    reads = []
    for k, g_all, vw, qc in sides:
        oy = bdot(g_all, vw)
        reads.append((oy[:, :128], (qc - oy[:, 128:]).astype(BF16)))
    bonus = dot(q * (sides[0][0] + sides[1][0]) * bonus_ref[...], ones) * val

    for j in order:
        copy(c1s.at[y], c1r.at[down(y, j)], x1s.at[j - 1], x1r.at[j - 1], "sp_1", y).wait_recv()
    side = y // 4
    both = jnp.where(iota((64, 128), 0) == (iota((64, 128), 1) & 63), 1.0, 0.0).astype(F32)
    joined = jnp.concatenate([both, jnp.zeros((16, 128), F32)], 0)
    fresh = jnp.zeros((64, 128), F32)
    prefixes = []
    for n in range(8):
        prefixes.append(joined)
        block = c1r[n + side * (7 - 2 * n)]
        joined = bdot(joined, expand(block[:64])) + jnp.concatenate(
            [fresh, block[64:].astype(F32)], 0
        )
    c2s[...] = joined.astype(BF16)
    c2r[z] = joined.astype(BF16)
    for j in order:
        go(copy(c2s, c2r.at[z], x2s.at[j - 1], x2r.at[j - 1], "sp_0", up(z, j)))

    def ring(s, start):
        last = s == 4
        first, second = (slice(0, 4), slice(4, 8)) if last else (slice(0, 8), slice(0, 8))
        n = down(z, s - 1) if start else down(z, s)
        m = up(z, s - 1) if start else up(z, s)
        u = down(y, s - 1) if start else down(y, s)
        v = up(y, s - 1) if start else up(y, s)
        four = (
            copy(wa.at[n, first], wa.at[n, first], a2s.at[0, s - 1], a2r.at[0, s - 1], "sp_0", up(z, 1)),
            copy(wa.at[m, second], wa.at[m, second], a2s.at[1, s - 1], a2r.at[1, s - 1], "sp_0", down(z, 1)),
            copy(wb.at[first, u], wb.at[first, u], b2s.at[0, s - 1], b2r.at[0, s - 1], "sp_1", up(y, 1)),
            copy(wb.at[second, v], wb.at[second, v], b2s.at[1, s - 1], b2r.at[1, s - 1], "sp_1", down(y, 1)),
        )
        for c in four:
            if start:
                go(c)
            else:
                c.wait_recv()

    for j in order:
        copy(wa_ref, wa.at[z, down(y, j)], a1s.at[j - 1], a1r.at[j - 1], "sp_1", y).wait_recv()
        copy(wb_ref, wb.at[down(z, j), y], b1s.at[j - 1], b1r.at[j - 1], "sp_0", z).wait_recv()
    ring(1, True)

    for j in order:
        copy(c2s, c2r.at[down(z, j)], x2s.at[j - 1], x2r.at[j - 1], "sp_0", z).wait_recv()
    entering = jnp.zeros((16, 128), F32)
    for n in range(8):
        at = n + side * (7 - 2 * n)
        block = c2r[at]
        new = bdot(entering, expand(block[:64])) + block[64:].astype(F32)
        before = (1 - 2 * side) * (z - at) > 0
        entering = jnp.where(before, new, entering)
    for n in range(8):
        before = prefixes[n]
        c3s[n + side * (7 - 2 * n)] = (
            bdot(entering, expand(before[:64])) + before[64:]
        ).astype(BF16)
    for j in order:
        w = up(y, j)
        go(copy(c3s.at[w], c3r.at[y], x3s.at[j - 1], x3r.at[j - 1], "sp_1", w))
    c3r[y] = c3s[y]

    for j in (1, 3, 2):
        at = 2 * down(xc, j, 4) + core
        copy(proj_ref, pb.at[at], p1s.at[j - 1], p1r.at[j - 1], "tp", tp).wait_recv()
        go(copy(pb.at[at], pb.at[at], p3s.at[j - 1], p3r.at[j - 1], "tp", partner))

    ring(1, False)
    ring(2, True)

    for j in order:
        copy(c3s.at[y], c3r.at[down(y, j)], x3s.at[j - 1], x3r.at[j - 1], "sp_1", y).wait_recv()
    summed = jnp.zeros((64, 128), F32)
    for d in range(2):
        state = jnp.concatenate([c3r[4 * d + part] for part in range(4)], 0)
        summed = summed + reads[d][0] + bdot(reads[d][1], expand(state), 1, 1)
    center = dot(summed, ones) * (1.0 / 64)
    away = summed - center
    spread = dot(away * away, ones) * (1.0 / 64)
    normed = away * lax.rsqrt(spread + GROUP_EPS) * again_ref[...]
    mixed = (normed + bonus) * valve_ref[...].astype(F32)
    mb[tp] = mixed.astype(BF16)
    for j in order:
        go(copy(mb.at[tp], mb.at[tp], ms.at[j - 1], mr.at[j - 1], "tp", up(tp, j)))
    copy(proj_ref, pb.at[partner], p2s.at[0], p2r.at[0], "tp", tp).wait_recv()
    for j in (1, 3, 2):
        at = 2 * down(xc, j, 4) + 1 - core
        copy(pb.at[at], pb.at[at], p3s.at[j - 1], p3r.at[j - 1], "tp", tp).wait_recv()
    for j in order:
        copy(mb.at[tp], mb.at[down(tp, j)], ms.at[j - 1], mr.at[j - 1], "tp", tp).wait_recv()

    rows = jnp.concatenate([mb[n] for n in range(8)], 1)

    def project(n, carry):
        cols = pl.ds(pl.multiple_of(n * 256, 256), 256)
        weights = pb[:, :, cols].reshape(1024, 256)
        midf[:, cols] = RESIDUAL_SCALE * skip_ref[:, cols].astype(F32) + bdot(rows, weights)
        return carry

    lax.fori_loop(0, 8, project, 0)

    def layer_norm(x, gain):
        center = jnp.mean(x, -1, keepdims=True)
        away = x - center
        spread = jnp.mean(away * away, -1, keepdims=True)
        return away * lax.rsqrt(spread + NORM_EPS) * gain

    for n in range(8):
        part = slice(8 * n, 8 * n + 8)
        normal = layer_norm(midf[part, :], mgain_ref[...]).astype(BF16)
        midf[part, :] = normal.astype(F32)
    midb[...] = midf[...].astype(BF16)

    ring(2, False)
    ring(3, True)
    ring(3, False)
    ring(4, True)
    ring(4, False)

    gu[...] = jnp.zeros_like(gu)

    def widen(n, carry):
        mid = midb[:, pl.ds(pl.multiple_of(n * 256, 256), 256)]
        gu[:, :1152] += bdot(mid, wa[n].reshape(256, 1152))
        gu[:, 1152:] += bdot(mid, wb[n, :, :, :256].reshape(256, 256))
        return carry

    lax.fori_loop(0, 8, widen, 0)

    gate, wide = gu[:, :640], gu[:, 640:1280]
    tail = gu[:, 1280:]
    main = gate / (1.0 + jnp.exp(-gate)) * wide
    rest = tail / (1.0 + jnp.exp(-tail)) * pltpu.roll(tail, 64, 1)
    rest = jnp.where(iota((64, 128), 1) < 64, rest, 0.0)
    inner = jnp.concatenate([main, rest], 1).astype(BF16)

    def shrink(n, carry):
        cols = pl.ds(pl.multiple_of(n * 256, 256), 256)
        share = bdot(inner, wb[n, :, :, 256:].reshape(256, 768), 1, 1)
        for m in range(8):
            rs[m, :, cols] = share[8 * m : 8 * m + 8].astype(BF16)
        return carry

    lax.fori_loop(0, 8, shrink, 0)
    for j in order:
        go(copy(rs.at[up(tp, j)], rr.at[tp], ds.at[j - 1], dr.at[j - 1], "tp", up(tp, j)))
    rr[tp] = rs[tp]
    for j in order:
        copy(rs.at[tp], rr.at[down(tp, j)], ds.at[j - 1], dr.at[j - 1], "tp", tp).wait_recv()
    total = RESIDUAL_SCALE * midf[pl.ds(pl.multiple_of(tp * 8, 8), 8), :]
    for n in range(8):
        total = total + rr[n].astype(F32)
    out_ref[...] = layer_norm(total, cgain_ref[...]).astype(BF16)
    for c in sent:
        c.wait_send()


def shards(
    skip, reading, labels, payloads, valve, fading, amend, extra, bonus, again, projector,
    mgain, gate, wide, shrink, cgain,
):
    down_rows = jnp.swapaxes(shrink, 0, 1)
    wa = jnp.concatenate([gate[:, :640], wide[:, :512]], 1)
    wb = jnp.concatenate(
        [wide[:, 512:640], gate[:, 640:], wide[:, 640:], down_rows, jnp.zeros((32, 64), BF16)], 1
    )
    fades = jnp.repeat(jnp.swapaxes(extra, 1, 2), 64, axis=2)
    dma = pltpu.SemaphoreType.DMA
    sems = [(7,)] * 4 + [(2, 4)] * 4 + [(3,), (3,), (1,), (1,), (3,), (3,)] + [(7,)] * 10
    return pl.pallas_call(
        body,
        out_shape=jax.ShapeDtypeStruct((8, 2048), BF16),
        in_specs=[pl.BlockSpec(memory_space=pltpu.VMEM)] * 15,
        out_specs=pl.BlockSpec(memory_space=pltpu.VMEM),
        scratch_shapes=[
            pltpu.VMEM((8, 8, 32, WA_COLS), BF16),
            pltpu.VMEM((8, 8, 32, WB_COLS), BF16),
            pltpu.VMEM((8, 128, 2048), BF16),
            pltpu.VMEM((8, 80, 128), BF16),
            pltpu.VMEM((8, 80, 128), BF16),
            pltpu.VMEM((80, 128), BF16),
            pltpu.VMEM((8, 80, 128), BF16),
            pltpu.VMEM((8, 16, 128), BF16),
            pltpu.VMEM((8, 16, 128), BF16),
            pltpu.VMEM((8, 64, 128), BF16),
            pltpu.VMEM((8, 8, 2048), BF16),
            pltpu.VMEM((8, 8, 2048), BF16),
            pltpu.VMEM((64, 2048), F32),
            pltpu.VMEM((64, 2048), BF16),
            pltpu.VMEM((64, 1408), F32),
        ]
        + [dma(s) for s in sems],
        compiler_params=pltpu.CompilerParams(
            collective_id=0, has_side_effects=True, vmem_limit_bytes=48 * 1024 * 1024
        ),
    )(
        skip, reading, labels, payloads, valve, fading, amend, fades, bonus.reshape(1, 128),
        again.reshape(1, 128), projector, mgain.reshape(1, 2048), wa, wb, cgain.reshape(1, 2048),
    )


def solution(mesh):
    finer = Mesh(mesh.devices.reshape(8, 8, mesh.shape["tp"]), ("sp_0", "sp_1", "tp"))
    placed = (
        P(SP, None),
        P(SP, "tp"),
        P(SP, "tp"),
        P(SP, "tp"),
        P(SP, "tp"),
        P(None, SP, "tp"),
        P(None, SP, "tp"),
        P(None, "tp", SP),
        P("tp"),
        P("tp"),
        P("tp", None),
        P(),
        P(SP, "tp"),
        P(SP, "tp"),
        P("tp", SP),
        P(),
    )
    return jax.shard_map(
        shards, mesh=finer, in_specs=placed, out_specs=P(SP_TP, None), check_vma=False
    )
```

time: 251 us -> 105 us (0.42)
  blocking collectives: 111 us -> 0 us
  Pallas kernels: 0 us -> 97.9 us
  matrix products: 57.5 us -> 0 us
  starting transfers between devices: 25.6 us -> 0 us
  other arithmetic: 24.8 us -> 0.01 us
  between operations: 14.1 us -> 0.18 us
  waiting for transfers between devices: 6.49 us -> 0 us
  local copies, waits for them, and re-layouts: 10.3 us -> 6.25 us
    pallas_call x0 -> x1, Pallas kernels: none -> 97.9 us  [shards(): pl.pallas_call(body, out_shape=jax.ShapeDtypeStruct((8, 2048), BF16), in_...]
    all_gather x4 -> x0, blocking collectives: 91.1 us -> none  [collected_together(): both, at, found = (lax.all_gather(jnp.concatenate(lines), axis), 0, {})]
    dot_general x184 -> x0, matrix products: 57.5 us -> none  [the longest x64 20.8 us: advance(): return (joined, jnp.einsum('hji,hj->hi', joined, query_vec))]
    all_to_all x1 -> x0, starting transfers between devices: 25.6 us -> none  [sent_and_summed(): lax.all_to_all(cut_along(value, dim, length), axis, 0, 0, tiled=True)]
    all_to_all x2 -> x0, blocking collectives: 19.8 us -> none  [the longest x1 9.91 us: sent_to_all(): return lax.all_to_all(copies, axis, split_axis=0, concat_axis=0, tiled=True)]
    add x16 -> x0, other arithmetic: 17.8 us -> none  [advance(): joined * decay_vec[:, :, None] + refill_vec[:, :, None] * erased[:, None, :]]
    all_to_all x1 -> x0, waiting for transfers between devices: 6.47 us -> none  [sent_and_summed(): lax.all_to_all(cut_along(value, dim, length), axis, 0, 0, tiled=True)]
    reduce_sum x10 -> x0, other arithmetic: 2.81 us -> none  [the longest x2 1.16 us: layer_norm(): spread = jnp.mean(jnp.square(summand - center), -1, keepdims=True)]
  transfers between devices with their start and end apart: 2 -> 0, of which waited for: 1 -> 0; matrix products, arithmetic and copies ran while one was open for 33% -> 0% of each run, Pallas kernels for 0% -> 0%
where the time goes in v1:
time: 105 us; the launch traced here: 104 us
  Pallas kernels  97.9 us (93%)
  local copies, waits for them, and re-layouts  6.25 us (6%)
    pallas_call x1, Pallas kernels, shards(): pl.pallas_call(body, out_shape=jax.ShapeDtypeStruct((8, 2048), BF16), in_...  97.9 us

profile of v1, /device:TPU:1, one launch (start us, length us, event | category | flops | bytes accessed | tf_op | source)
XLA Modules:
  0.0 104.4 jit_solution(16239167224074877173)
XLA Ops:
  0.0 0.8 copy.17
  0.8 0.2 broadcast_in_dim.6
  1.0 0.0 slice-start
  1.1 0.1 reshape.15.extra_ref
  1.2 0.8 slice.15
  2.0 0.0 slice-done
  2.0 0.7 slice.17
  2.7 0.7 slice.18
  3.4 0.7 slice.19
  4.1 0.0 copy-start.4
  4.2 0.0 copy-start.5
  4.2 0.0 copy-start.6
  4.2 0.0 copy-start.7
  4.2 0.0 copy-start.8
  4.2 0.0 copy-start.9
  4.2 0.9 concatenate.7.wb_ref
  5.1 0.0 copy-start.10
  5.2 0.0 copy-start.11
  5.2 0.0 copy-done
  5.2 0.0 copy-done.1
  5.2 0.0 copy-done.2
  5.2 0.0 copy-done.3
  5.2 0.0 copy-done.4
  5.2 0.0 copy-done.5
  5.2 0.0 copy-done.6
  5.2 0.0 copy-done.7
  5.2 0.0 copy-done.8
  5.3 0.0 copy-done.9
  5.3 0.5 copy-done.10
  5.8 0.0 copy-done.11
  5.8 97.9 %shard_map.154 = bf16[8,2048]{1,0:T(8,128)(2,1)S(1)} custom-call(bf16[64,2048]{1,0:T(8,128)(2,1)S(1)} %copy-done.1, bf16[64,128]{1,0:T(8,128)(2,1)S(1)} %copy-done.4, bf16[64,128]{1,0:T(8,128)(2,1)S(1)} %copy-done.5, bf16[64,128]{1,0:T(8,128)(2,1)S(1)} %copy-done.6, bf16[64,128]{1,0:T(8,128)(2,1)S(1)} %copy-done.7, bf16[2,64,128]{2,1,0:T(8,128)(2,1)S(1)} %copy-done.2, ...), custom_call_target="tpu_custom_call" | custom-call | tf_op jit(solution)/shard_map/pallas_call | solution.py:335
  103.8 0.6 copy.19
  (6 shorter events, 0.0 us)
Async XLA Ops:
  0.0 5.2 %copy-start = (bf16[128,2048]{1,0:T(8,128)(2,1)S(1)}, bf16[128,2048]{1,0:T(8,128)(2,1)}, u32[]{:S(2)}) copy-start(bf16[128,2048]{1,0:T(8,128)(2,1)} %proj_ref.1) | copy-start | bytes 1572868
  1.0 1.0 slice-start
  1.2 4.0 %copy-start.1 = (bf16[64,2048]{1,0:T(8,128)(2,1)S(1)}, bf16[64,2048]{1,0:T(8,128)(2,1)}, u32[]{:S(2)}) copy-start(bf16[64,2048]{1,0:T(8,128)(2,1)} %skip_ref.1) | copy-start | bytes 786436
  4.1 1.1 %copy-start.2 = (bf16[2,64,128]{2,1,0:T(8,128)(2,1)S(1)}, bf16[2,64,128]{2,1,0:T(8,128)(2,1)}, u32[]{:S(2)}) copy-start(bf16[2,64,128]{2,1,0:T(8,128)(2,1)} %fade_ref.1) | copy-start | bytes 98308
  4.1 1.1 %copy-start.3 = (bf16[2,64,128]{2,1,0:T(8,128)(2,1)S(1)}, bf16[2,64,128]{2,1,0:T(8,128)(2,1)}, u32[]{:S(2)}) copy-start(bf16[2,64,128]{2,1,0:T(8,128)(2,1)} %amend_ref.1) | copy-start | bytes 98308
  4.1 1.1 %copy-start.4 = (bf16[64,128]{1,0:T(8,128)(2,1)S(1)}, bf16[64,128]{1,0:T(8,128)(2,1)}, u32[]{:S(2)}) copy-start(bf16[64,128]{1,0:T(8,128)(2,1)} %q_ref.1) | copy-start | bytes 49156
  4.2 1.1 %copy-start.5 = (bf16[64,128]{1,0:T(8,128)(2,1)S(1)}, bf16[64,128]{1,0:T(8,128)(2,1)}, u32[]{:S(2)}) copy-start(bf16[64,128]{1,0:T(8,128)(2,1)} %key_ref.1) | copy-start | bytes 49156
  4.2 1.1 %copy-start.6 = (bf16[64,128]{1,0:T(8,128)(2,1)S(1)}, bf16[64,128]{1,0:T(8,128)(2,1)}, u32[]{:S(2)}) copy-start(bf16[64,128]{1,0:T(8,128)(2,1)} %val_ref.1) | copy-start | bytes 49156
  4.2 1.1 %copy-start.7 = (bf16[64,128]{1,0:T(8,128)(2,1)S(1)}, bf16[64,128]{1,0:T(8,128)(2,1)}, u32[]{:S(2)}) copy-start(bf16[64,128]{1,0:T(8,128)(2,1)} %valve_ref.1) | copy-start | bytes 49156
  4.2 1.1 %copy-start.8 = (f32[2048]{0:T(1024)S(1)}, f32[2048]{0:T(1024)}, u32[]{:S(2)}) copy-start(f32[2048]{0:T(1024)} %param.27) | copy-start | bytes 24580
  4.2 1.1 %copy-start.9 = (f32[2048]{0:T(1024)S(1)}, f32[2048]{0:T(1024)}, u32[]{:S(2)}) copy-start(f32[2048]{0:T(1024)} %param.31) | copy-start | bytes 24580
  5.1 0.7 copy-start.10
  5.2 0.7 copy-start.11

commit v2 on v1

--- a/solution.py
+++ b/solution.py
@@ -23,6 +23,7 @@
 LANES = 128
 WA_COLS = 1152
 WB_COLS = 1024
+PIECES = ((0, 1, 7, 2), (6, 3, 5, 4))
 
 
 def dot(a, b, ca=1, cb=0):
@@ -96,11 +97,13 @@
 
 
 def body(
+    skip_hbm, q_hbm, key_hbm, val_hbm, valve_hbm, fade_hbm, amend_hbm, extra_hbm, bonus_hbm,
+    again_hbm, proj_hbm, mgain_hbm, gate_hbm, wide_hbm, drow_hbm, cgain_hbm, out_ref,
     skip_ref, q_ref, key_ref, val_ref, valve_ref, fade_ref, amend_ref, extra_ref, bonus_ref,
-    again_ref, proj_ref, mgain_ref, wa_ref, wb_ref, cgain_ref, out_ref,
+    again_ref, mgain_ref, gate_ref, wide_ref, drow_ref, cgain_ref,
     wa, wb, pb, c1s, c1r, c2s, c2r, c3s, c3r, mb, rs, rr, midf, midb, gu,
     a1s, a1r, b1s, b1r, a2s, a2r, b2s, b2r, p1s, p1r, p2s, p2r, p3s, p3r,
-    x1s, x1r, x2s, x2r, x3s, x3r, ms, mr, ds, dr,
+    x1s, x1r, x2s, x2r, x3s, x3r, ms, mr, ds, dr, early, weighty, late,
 ):
     z, y, tp = lax.axis_index("sp_0"), lax.axis_index("sp_1"), lax.axis_index("tp")
     xc, core = tp // 2, tp % 2
@@ -122,47 +125,119 @@
     for axis, at in (("sp_0", z), ("sp_1", y), ("tp", tp)):
         for j in range(1, 8):
             pl.semaphore_signal(barrier, inc=1, device_id={axis: up(at, j)}, device_id_type=MESH)
-    pl.semaphore_wait(barrier, 21)
-
+
+    def fetch(pairs, sem):
+        copies = [pltpu.make_async_copy(a, b, sem.at[n]) for n, (a, b) in enumerate(pairs)]
+        for c in copies:
+            c.start()
+        return copies
+
+    early_copies = fetch(
+        (
+            (key_hbm, key_ref), (fade_hbm, fade_ref), (amend_hbm, amend_ref), (extra_hbm, extra_ref),
+            (q_hbm, q_ref), (val_hbm, val_ref),
+        ),
+        early,
+    )
+    weight_copies = fetch(
+        ((gate_hbm, gate_ref), (wide_hbm, wide_ref), (drow_hbm, drow_ref), (proj_hbm, pb.at[tp])), weighty
+    )
+    late_copies = fetch(
+        (
+            (valve_hbm, valve_ref), (bonus_hbm, bonus_ref), (again_hbm, again_ref),
+            (skip_hbm, skip_ref), (mgain_hbm, mgain_ref), (cgain_hbm, cgain_ref),
+        ),
+        late,
+    )
     sent = []
+    order = (1, 7, 2, 6, 3, 5, 4)
 
     def go(c):
         c.start()
         sent.append(c)
 
-    order = (1, 7, 2, 6, 3, 5, 4)
-    for j in order:
-        go(copy(wa_ref, wa.at[z, y], a1s.at[j - 1], a1r.at[j - 1], "sp_1", up(y, j)))
-        go(copy(wb_ref, wb.at[z, y], b1s.at[j - 1], b1r.at[j - 1], "sp_0", up(z, j)))
-    for j in (1, 3, 2):
-        go(copy(proj_ref, pb.at[tp], p1s.at[j - 1], p1r.at[j - 1], "tp", 2 * up(xc, j, 4) + core))
-    go(copy(proj_ref, pb.at[tp], p2s.at[0], p2r.at[0], "tp", partner))
-    wa[z, y] = wa_ref[...]
-    wb[z, y] = wb_ref[...]
-    pb[tp] = proj_ref[...]
-
+    for c in early_copies:
+        c.wait()
     q, key, val = q_ref[...].astype(F32), key_ref[...].astype(F32), val_ref[...].astype(F32)
     ones = head_ones()
+    spread_heads = jnp.where((iota((2, 128), 1) >> 6) == iota((2, 128), 0), 1.0, 0.0).astype(F32)
     inv = lax.rsqrt(dot(key * key, ones) + KEY_EPS)
     sides = []
     for d in range(2):
         k, passed, written, g_all, vw, qc = local_mixer(
-            q, key, val, inv, fade_ref[d].astype(F32), amend_ref[d].astype(F32), extra_ref[d], d
+            q, key, val, inv, fade_ref[d].astype(F32), amend_ref[d].astype(F32),
+            dot(extra_ref[d], spread_heads, 0, 0), d
         )
         passed, written = passed.astype(BF16), written.astype(BF16)
         for part in range(4):
             c1s[4 * d + part] = jnp.concatenate([passed, written[16 * part : 16 * part + 16]], 0)
         sides.append((k, g_all, vw, qc))
+    for c in weight_copies:
+        c.wait()
+    wa[z, y] = jnp.concatenate([gate_ref[:, :640], wide_ref[:, :512]], 1)
+    wb[z, y, :, :128] = wide_ref[:, 512:640]
+    wb[z, y, :, 128:256] = jnp.concatenate([gate_ref[:, 640:], wide_ref[:, 640:]], 1)
+    wb[z, y, :, 256:896] = drow_ref[:, :640]
+    wb[z, y, :, 896:] = jnp.concatenate([drow_ref[:, 640:], jnp.zeros((32, 64), BF16)], 1)
+    pl.semaphore_wait(barrier, 21)
     for j in order:
         w = up(y, j)
         go(copy(c1s.at[w], c1r.at[y], x1s.at[j - 1], x1r.at[j - 1], "sp_1", w))
     c1r[y] = c1s[y]
 
+    def first_a(j, block, target, part=slice(0, 32), sem=None):
+        sem = j - 1 if sem is None else sem
+        return copy(wa.at[z, block, part], wa.at[z, block, part], a1s.at[sem], a1r.at[sem], "sp_1", target)
+
+    def first_b(j, block, target, part=slice(0, 32), sem=None):
+        sem = j - 1 if sem is None else sem
+        return copy(wb.at[block, y, part], wb.at[block, y, part], b1s.at[sem], b1r.at[sem], "sp_0", target)
+
+    for j in (1, 7, 2, 6):
+        go(first_a(j, y, up(y, j)))
+        go(first_b(j, z, up(z, j)))
+    for j in (1, 3, 2):
+        go(copy(pb.at[tp], pb.at[tp], p1s.at[j - 1], p1r.at[j - 1], "tp", 2 * up(xc, j, 4) + core))
+    go(copy(pb.at[tp], pb.at[tp], p2s.at[0], p2r.at[0], "tp", partner))
+
+    for c in late_copies:
+        c.wait()
     reads = []
     for k, g_all, vw, qc in sides:
         oy = bdot(g_all, vw)
         reads.append((oy[:, :128], (qc - oy[:, 128:]).astype(BF16)))
     bonus = dot(q * (sides[0][0] + sides[1][0]) * bonus_ref[...], ones) * val
+
+    for first, at in ((first_a, y), (first_b, z)):
+        for j in (1, 7, 2, 6):
+            first(j, down(at, j), at).wait_recv()
+        go(first(3, down(at, 2), up(at, 1)))
+        go(first(5, up(at, 2), down(at, 1)))
+        go(first(4, down(at, 2), up(at, 2), slice(0, 16)))
+        go(first(4, up(at, 2), down(at, 2), slice(16, 32), 7))
+
+    held = []
+
+    def ring(s, p, start):
+        for way in range(2):
+            if s == 4 and way != p:
+                continue
+            back, on = (down, up) if way == 0 else (up, down)
+            a_sems = a2s.at[way, s - 1, p], a2r.at[way, s - 1, p]
+            b_sems = b2s.at[way, s - 1, p], b2r.at[way, s - 1, p]
+            if start:
+                n, m = back(z, s - 1), back(y, s - 1)
+                for e in PIECES[p]:
+                    a, b = wa.at[n, up(y, e)], wb.at[up(z, e), m]
+                    copy(a, a, *a_sems, "sp_0", on(z, 1)).start()
+                    copy(b, b, *b_sems, "sp_1", on(y, 1)).start()
+                held.append(copy(wa.at[0, 0:4], wa.at[0, 0:4], *a_sems, "sp_0", z))
+                held.append(copy(wb.at[0, 0:4], wb.at[0, 0:4], *b_sems, "sp_1", y))
+            else:
+                copy(wa.at[0, 0:4], wa.at[0, 0:4], *a_sems, "sp_0", z).wait_recv()
+                copy(wb.at[0, 0:4], wb.at[0, 0:4], *b_sems, "sp_1", y).wait_recv()
+
+    ring(1, 0, True)
 
     for j in order:
         copy(c1s.at[y], c1r.at[down(y, j)], x1s.at[j - 1], x1r.at[j - 1], "sp_1", y).wait_recv()
@@ -182,29 +257,14 @@
     for j in order:
         go(copy(c2s, c2r.at[z], x2s.at[j - 1], x2r.at[j - 1], "sp_0", up(z, j)))
 
-    def ring(s, start):
-        last = s == 4
-        first, second = (slice(0, 4), slice(4, 8)) if last else (slice(0, 8), slice(0, 8))
-        n = down(z, s - 1) if start else down(z, s)
-        m = up(z, s - 1) if start else up(z, s)
-        u = down(y, s - 1) if start else down(y, s)
-        v = up(y, s - 1) if start else up(y, s)
-        four = (
-            copy(wa.at[n, first], wa.at[n, first], a2s.at[0, s - 1], a2r.at[0, s - 1], "sp_0", up(z, 1)),
-            copy(wa.at[m, second], wa.at[m, second], a2s.at[1, s - 1], a2r.at[1, s - 1], "sp_0", down(z, 1)),
-            copy(wb.at[first, u], wb.at[first, u], b2s.at[0, s - 1], b2r.at[0, s - 1], "sp_1", up(y, 1)),
-            copy(wb.at[second, v], wb.at[second, v], b2s.at[1, s - 1], b2r.at[1, s - 1], "sp_1", down(y, 1)),
-        )
-        for c in four:
-            if start:
-                go(c)
-            else:
-                c.wait_recv()
-
-    for j in order:
-        copy(wa_ref, wa.at[z, down(y, j)], a1s.at[j - 1], a1r.at[j - 1], "sp_1", y).wait_recv()
-        copy(wb_ref, wb.at[down(z, j), y], b1s.at[j - 1], b1r.at[j - 1], "sp_0", z).wait_recv()
-    ring(1, True)
+    for first, at in ((first_a, y), (first_b, z)):
+        first(3, down(at, 3), at).wait_recv()
+        first(5, up(at, 3), at).wait_recv()
+        first(4, up(at, 4), at, slice(0, 16)).wait_recv()
+        first(4, up(at, 4), at, slice(16, 32), 7).wait_recv()
+    ring(1, 1, True)
+    ring(1, 0, False)
+    ring(2, 0, True)
 
     for j in order:
         copy(c2s, c2r.at[down(z, j)], x2s.at[j - 1], x2r.at[j - 1], "sp_0", z).wait_recv()
@@ -227,11 +287,13 @@
 
     for j in (1, 3, 2):
         at = 2 * down(xc, j, 4) + core
-        copy(proj_ref, pb.at[at], p1s.at[j - 1], p1r.at[j - 1], "tp", tp).wait_recv()
+        copy(pb.at[tp], pb.at[at], p1s.at[j - 1], p1r.at[j - 1], "tp", tp).wait_recv()
         go(copy(pb.at[at], pb.at[at], p3s.at[j - 1], p3r.at[j - 1], "tp", partner))
 
-    ring(1, False)
-    ring(2, True)
+    ring(1, 1, False)
+    ring(2, 1, True)
+    ring(2, 0, False)
+    ring(3, 0, True)
 
     for j in order:
         copy(c3s.at[y], c3r.at[down(y, j)], x3s.at[j - 1], x3r.at[j - 1], "sp_1", y).wait_recv()
@@ -247,7 +309,9 @@
     mb[tp] = mixed.astype(BF16)
     for j in order:
         go(copy(mb.at[tp], mb.at[tp], ms.at[j - 1], mr.at[j - 1], "tp", up(tp, j)))
-    copy(proj_ref, pb.at[partner], p2s.at[0], p2r.at[0], "tp", tp).wait_recv()
+    ring(2, 1, False)
+    ring(3, 1, True)
+    copy(pb.at[tp], pb.at[partner], p2s.at[0], p2r.at[0], "tp", tp).wait_recv()
     for j in (1, 3, 2):
         at = 2 * down(xc, j, 4) + 1 - core
         copy(pb.at[at], pb.at[at], p3s.at[j - 1], p3r.at[j - 1], "tp", tp).wait_recv()
@@ -276,21 +340,31 @@
         midf[part, :] = normal.astype(F32)
     midb[...] = midf[...].astype(BF16)
 
-    ring(2, False)
-    ring(3, True)
-    ring(3, False)
-    ring(4, True)
-    ring(4, False)
+    ring(3, 0, False)
+    ring(4, 0, True)
+    ring(3, 1, False)
+    ring(4, 1, True)
 
     gu[...] = jnp.zeros_like(gu)
 
-    def widen(n, carry):
+    def widen(n):
         mid = midb[:, pl.ds(pl.multiple_of(n * 256, 256), 256)]
         gu[:, :1152] += bdot(mid, wa[n].reshape(256, 1152))
+
+    def widen_near(n, carry):
+        widen(up(z, n + 5))
+        return carry
+
+    def widen_rest(n, carry):
+        mid = midb[:, pl.ds(pl.multiple_of(n * 256, 256), 256)]
         gu[:, 1152:] += bdot(mid, wb[n, :, :, :256].reshape(256, 256))
         return carry
 
-    lax.fori_loop(0, 8, widen, 0)
+    lax.fori_loop(0, 7, widen_near, 0)
+    ring(4, 0, False)
+    ring(4, 1, False)
+    widen(up(z, 4))
+    lax.fori_loop(0, 8, widen_rest, 0)
 
     gate, wide = gu[:, :640], gu[:, 640:1280]
     tail = gu[:, 1280:]
@@ -316,7 +390,7 @@
     for n in range(8):
         total = total + rr[n].astype(F32)
     out_ref[...] = layer_norm(total, cgain_ref[...]).astype(BF16)
-    for c in sent:
+    for c in sent + held:
         c.wait_send()
 
 
@@ -325,19 +399,29 @@
     mgain, gate, wide, shrink, cgain,
 ):
     down_rows = jnp.swapaxes(shrink, 0, 1)
-    wa = jnp.concatenate([gate[:, :640], wide[:, :512]], 1)
-    wb = jnp.concatenate(
-        [wide[:, 512:640], gate[:, 640:], wide[:, 640:], down_rows, jnp.zeros((32, 64), BF16)], 1
-    )
-    fades = jnp.repeat(jnp.swapaxes(extra, 1, 2), 64, axis=2)
     dma = pltpu.SemaphoreType.DMA
-    sems = [(7,)] * 4 + [(2, 4)] * 4 + [(3,), (3,), (1,), (1,), (3,), (3,)] + [(7,)] * 10
+    sems = [(8,)] * 4 + [(2, 4, 2)] * 4 + [(3,), (3,), (1,), (1,), (3,), (3,)] + [(7,)] * 10 + [(6,), (4,), (6,)]
     return pl.pallas_call(
         body,
         out_shape=jax.ShapeDtypeStruct((8, 2048), BF16),
-        in_specs=[pl.BlockSpec(memory_space=pltpu.VMEM)] * 15,
+        in_specs=[pl.BlockSpec(memory_space=pltpu.HBM)] * 16,
         out_specs=pl.BlockSpec(memory_space=pltpu.VMEM),
         scratch_shapes=[
+            pltpu.VMEM((64, 2048), BF16),
+            pltpu.VMEM((64, 128), BF16),
+            pltpu.VMEM((64, 128), BF16),
+            pltpu.VMEM((64, 128), BF16),
+            pltpu.VMEM((64, 128), BF16),
+            pltpu.VMEM((2, 64, 128), BF16),
+            pltpu.VMEM((2, 64, 128), BF16),
+            pltpu.VMEM((2, 2, 64), F32),
+            pltpu.VMEM((1, 128), F32),
+            pltpu.VMEM((1, 128), F32),
+            pltpu.VMEM((1, 2048), F32),
+            pltpu.VMEM((32, 704), BF16),
+            pltpu.VMEM((32, 704), BF16),
+            pltpu.VMEM((32, 704), BF16),
+            pltpu.VMEM((1, 2048), F32),
             pltpu.VMEM((8, 8, 32, WA_COLS), BF16),
             pltpu.VMEM((8, 8, 32, WB_COLS), BF16),
             pltpu.VMEM((8, 128, 2048), BF16),
@@ -356,11 +440,12 @@
         ]
         + [dma(s) for s in sems],
         compiler_params=pltpu.CompilerParams(
-            collective_id=0, has_side_effects=True, vmem_limit_bytes=48 * 1024 * 1024
+            collective_id=0, has_side_effects=True, vmem_limit_bytes=67043328
         ),
     )(
-        skip, reading, labels, payloads, valve, fading, amend, fades, bonus.reshape(1, 128),
-        again.reshape(1, 128), projector, mgain.reshape(1, 2048), wa, wb, cgain.reshape(1, 2048),
+        skip, reading, labels, payloads, valve, fading, amend, extra, bonus.reshape(1, 128),
+        again.reshape(1, 128), projector, mgain.reshape(1, 2048), gate, wide,
+        down_rows, cgain.reshape(1, 2048),
     )
 
 

time: 105 us -> 94.9 us (0.904)
  local copies, waits for them, and re-layouts: 6.25 us -> 1.38 us
  Pallas kernels: 97.9 us -> 93.3 us
    pallas_call x1, Pallas kernels: 97.9 us -> 93.3 us  [shards(): pl.pallas_call(body, out_shape=jax.ShapeDtypeStruct((8, 2048), BF16), in_...]
    slice x6 -> x0, local copies, waits for them, and re-layouts: 2.93 us -> none  [the longest x3 0.83 us: shards(): wa = jnp.concatenate([gate[:, :640], wide[:, :512]], 1)]
where the time goes in v2:
time: 94.9 us; the launch traced here: 94.7 us
  Pallas kernels  93.3 us (98%)
  local copies, waits for them, and re-layouts  1.38 us (1%)
    pallas_call x1, Pallas kernels, shards(): pl.pallas_call(body, out_shape=jax.ShapeDtypeStruct((8, 2048), BF16), in_...  93.3 us

profile of v2, /device:TPU:1, one launch (start us, length us, event | category | flops | bytes accessed | tf_op | source)
XLA Modules:
  0.0 94.7 jit_solution(5752030517086260013)
XLA Ops:
  0.0 93.3 %shard_map.154 = bf16[8,2048]{1,0:T(8,128)(2,1)} custom-call(bf16[64,2048]{1,0:T(8,128)(2,1)} %skip_hbm.1, bf16[64,128]{1,0:T(8,128)(2,1)} %q_hbm.1, bf16[64,128]{1,0:T(8,128)(2,1)} %key_hbm.1, bf16[64,128]{1,0:T(8,128)(2,1)} %val_hbm.1, bf16[64,128]{1,0:T(8,128)(2,1)} %valve_hbm.1, bf16[2,64,128]{2,1,0:T(8,128)(2,1)} %fade_hbm.1, ...), custom_call_target="tpu_custom_call" | custom-call | tf_op jit(solution)/shard_map/pallas_call | solution.py:404
  93.3 1.4 %copy.18 = bf16[8,2048]{1,0:T(8,128)(2,1)} copy(bf16[8,2048]{1,0:T(8,128)(2,1)} %shard_map.154) | data formatting | bytes 65536

commit v3 on v2

--- a/solution.py
+++ b/solution.py
@@ -23,7 +23,7 @@
 LANES = 128
 WA_COLS = 1152
 WB_COLS = 1024
-PIECES = ((0, 1, 7, 2), (6, 3, 5, 4))
+PIECES = ((0, 1, 7), (2, 6), (3, 5, 4))
 
 
 def dot(a, b, ca=1, cb=0):
@@ -180,25 +180,70 @@
     wb[z, y, :, 256:896] = drow_ref[:, :640]
     wb[z, y, :, 896:] = jnp.concatenate([drow_ref[:, 640:], jnp.zeros((32, 64), BF16)], 1)
     pl.semaphore_wait(barrier, 21)
+    def first(k, start):
+        for way in range(2):
+            back, on = (down, up) if way == 0 else (up, down)
+            part = slice(0, 32) if k < 4 else slice(16 * way, 16 * way + 16)
+            at = k - 1 if start else k
+            a, b = wa.at[z, back(y, at), part], wb.at[back(z, at), y, part]
+            a = copy(a, a, a1s.at[way, k - 1], a1r.at[way, k - 1], "sp_1", on(y, 1))
+            b = copy(b, b, b1s.at[way, k - 1], b1r.at[way, k - 1], "sp_0", on(z, 1))
+            if start:
+                go(a)
+                go(b)
+            else:
+                a.wait_recv()
+                b.wait_recv()
+
+    held = []
+
+    def piece(s, p, way):
+        if s < 4:
+            return PIECES[p]
+        return (((0, 1, 7), (2,), ()), ((), (6,), (3, 5, 4)))[way][p]
+
+    def ring_sems(s, p, way):
+        return (a2s.at[way, s - 1, p], a2r.at[way, s - 1, p]), (b2s.at[way, s - 1, p], b2r.at[way, s - 1, p])
+
+    def whole(s, p, way):
+        n = len(piece(s, p, way))
+        a_sems, b_sems = ring_sems(s, p, way)
+        return (
+            copy(wa.at[0, 0:n], wa.at[0, 0:n], *a_sems, "sp_0", z),
+            copy(wb.at[0, 0:n], wb.at[0, 0:n], *b_sems, "sp_1", y),
+        )
+
+    def send(s, p, only=None):
+        for way in range(2):
+            back, on = (down, up) if way == 0 else (up, down)
+            a_sems, b_sems = ring_sems(s, p, way)
+            n, m = back(z, s - 1), back(y, s - 1)
+            for e in piece(s, p, way) if only is None else only:
+                a, b = wa.at[n, up(y, e)], wb.at[up(z, e), m]
+                copy(a, a, *a_sems, "sp_0", on(z, 1)).start()
+                copy(b, b, *b_sems, "sp_1", on(y, 1)).start()
+            if piece(s, p, way) and (only is None or only[-1] == PIECES[p][-1]):
+                held.extend(whole(s, p, way))
+
+    def take(s, p):
+        for way in range(2):
+            if piece(s, p, way):
+                for c in whole(s, p, way):
+                    c.wait_recv()
+
+    first(1, True)
+    send(1, 0, (0,))
     for j in order:
         w = up(y, j)
         go(copy(c1s.at[w], c1r.at[y], x1s.at[j - 1], x1r.at[j - 1], "sp_1", w))
     c1r[y] = c1s[y]
-
-    def first_a(j, block, target, part=slice(0, 32), sem=None):
-        sem = j - 1 if sem is None else sem
-        return copy(wa.at[z, block, part], wa.at[z, block, part], a1s.at[sem], a1r.at[sem], "sp_1", target)
-
-    def first_b(j, block, target, part=slice(0, 32), sem=None):
-        sem = j - 1 if sem is None else sem
-        return copy(wb.at[block, y, part], wb.at[block, y, part], b1s.at[sem], b1r.at[sem], "sp_0", target)
-
-    for j in (1, 7, 2, 6):
-        go(first_a(j, y, up(y, j)))
-        go(first_b(j, z, up(z, j)))
     for j in (1, 3, 2):
         go(copy(pb.at[tp], pb.at[tp], p1s.at[j - 1], p1r.at[j - 1], "tp", 2 * up(xc, j, 4) + core))
     go(copy(pb.at[tp], pb.at[tp], p2s.at[0], p2r.at[0], "tp", partner))
+
+    first(1, False)
+    first(2, True)
+    send(1, 0, (1, 7))
 
     for c in late_copies:
         c.wait()
@@ -208,36 +253,9 @@
         reads.append((oy[:, :128], (qc - oy[:, 128:]).astype(BF16)))
     bonus = dot(q * (sides[0][0] + sides[1][0]) * bonus_ref[...], ones) * val
 
-    for first, at in ((first_a, y), (first_b, z)):
-        for j in (1, 7, 2, 6):
-            first(j, down(at, j), at).wait_recv()
-        go(first(3, down(at, 2), up(at, 1)))
-        go(first(5, up(at, 2), down(at, 1)))
-        go(first(4, down(at, 2), up(at, 2), slice(0, 16)))
-        go(first(4, up(at, 2), down(at, 2), slice(16, 32), 7))
-
-    held = []
-
-    def ring(s, p, start):
-        for way in range(2):
-            if s == 4 and way != p:
-                continue
-            back, on = (down, up) if way == 0 else (up, down)
-            a_sems = a2s.at[way, s - 1, p], a2r.at[way, s - 1, p]
-            b_sems = b2s.at[way, s - 1, p], b2r.at[way, s - 1, p]
-            if start:
-                n, m = back(z, s - 1), back(y, s - 1)
-                for e in PIECES[p]:
-                    a, b = wa.at[n, up(y, e)], wb.at[up(z, e), m]
-                    copy(a, a, *a_sems, "sp_0", on(z, 1)).start()
-                    copy(b, b, *b_sems, "sp_1", on(y, 1)).start()
-                held.append(copy(wa.at[0, 0:4], wa.at[0, 0:4], *a_sems, "sp_0", z))
-                held.append(copy(wb.at[0, 0:4], wb.at[0, 0:4], *b_sems, "sp_1", y))
-            else:
-                copy(wa.at[0, 0:4], wa.at[0, 0:4], *a_sems, "sp_0", z).wait_recv()
-                copy(wb.at[0, 0:4], wb.at[0, 0:4], *b_sems, "sp_1", y).wait_recv()
-
-    ring(1, 0, True)
+    first(2, False)
+    first(3, True)
+    send(1, 1)
 
     for j in order:
         copy(c1s.at[y], c1r.at[down(y, j)], x1s.at[j - 1], x1r.at[j - 1], "sp_1", y).wait_recv()
@@ -257,14 +275,15 @@
     for j in order:
         go(copy(c2s, c2r.at[z], x2s.at[j - 1], x2r.at[j - 1], "sp_0", up(z, j)))
 
-    for first, at in ((first_a, y), (first_b, z)):
-        first(3, down(at, 3), at).wait_recv()
-        first(5, up(at, 3), at).wait_recv()
-        first(4, up(at, 4), at, slice(0, 16)).wait_recv()
-        first(4, up(at, 4), at, slice(16, 32), 7).wait_recv()
-    ring(1, 1, True)
-    ring(1, 0, False)
-    ring(2, 0, True)
+    first(3, False)
+    first(4, True)
+    send(1, 2, (3, 5))
+    take(1, 0)
+    send(2, 0)
+    first(4, False)
+    send(1, 2, (4,))
+    take(1, 1)
+    send(2, 1)
 
     for j in order:
         copy(c2s, c2r.at[down(z, j)], x2s.at[j - 1], x2r.at[j - 1], "sp_0", z).wait_recv()
@@ -285,15 +304,18 @@
         go(copy(c3s.at[w], c3r.at[y], x3s.at[j - 1], x3r.at[j - 1], "sp_1", w))
     c3r[y] = c3s[y]
 
+    take(1, 2)
+    send(2, 2)
+    take(2, 0)
+    send(3, 0)
+
     for j in (1, 3, 2):
         at = 2 * down(xc, j, 4) + core
         copy(pb.at[tp], pb.at[at], p1s.at[j - 1], p1r.at[j - 1], "tp", tp).wait_recv()
         go(copy(pb.at[at], pb.at[at], p3s.at[j - 1], p3r.at[j - 1], "tp", partner))
 
-    ring(1, 1, False)
-    ring(2, 1, True)
-    ring(2, 0, False)
-    ring(3, 0, True)
+    take(2, 1)
+    send(3, 1)
 
     for j in order:
         copy(c3s.at[y], c3r.at[down(y, j)], x3s.at[j - 1], x3r.at[j - 1], "sp_1", y).wait_recv()
@@ -309,8 +331,8 @@
     mb[tp] = mixed.astype(BF16)
     for j in order:
         go(copy(mb.at[tp], mb.at[tp], ms.at[j - 1], mr.at[j - 1], "tp", up(tp, j)))
-    ring(2, 1, False)
-    ring(3, 1, True)
+    take(2, 2)
+    send(3, 2)
     copy(pb.at[tp], pb.at[partner], p2s.at[0], p2r.at[0], "tp", tp).wait_recv()
     for j in (1, 3, 2):
         at = 2 * down(xc, j, 4) + 1 - core
@@ -340,10 +362,12 @@
         midf[part, :] = normal.astype(F32)
     midb[...] = midf[...].astype(BF16)
 
-    ring(3, 0, False)
-    ring(4, 0, True)
-    ring(3, 1, False)
-    ring(4, 1, True)
+    take(3, 0)
+    send(4, 0)
+    take(3, 1)
+    send(4, 1)
+    take(3, 2)
+    send(4, 2)
 
     gu[...] = jnp.zeros_like(gu)
 
@@ -361,8 +385,9 @@
         return carry
 
     lax.fori_loop(0, 7, widen_near, 0)
-    ring(4, 0, False)
-    ring(4, 1, False)
+    take(4, 0)
+    take(4, 1)
+    take(4, 2)
     widen(up(z, 4))
     lax.fori_loop(0, 8, widen_rest, 0)
 
@@ -380,12 +405,20 @@
             rs[m, :, cols] = share[8 * m : 8 * m + 8].astype(BF16)
         return carry
 
-    lax.fori_loop(0, 8, shrink, 0)
-    for j in order:
-        go(copy(rs.at[up(tp, j)], rr.at[tp], ds.at[j - 1], dr.at[j - 1], "tp", up(tp, j)))
+    def share_copy(half, j, source, target):
+        cols = slice(1024 * half, 1024 * half + 1024)
+        return copy(
+            rs.at[target, :, cols], rr.at[source, :, cols], ds.at[half, j - 1], dr.at[half, j - 1], "tp", target
+        )
+
+    for half in range(2):
+        lax.fori_loop(4 * half, 4 * half + 4, shrink, 0)
+        for j in order:
+            go(share_copy(half, j, tp, up(tp, j)))
     rr[tp] = rs[tp]
-    for j in order:
-        copy(rs.at[tp], rr.at[down(tp, j)], ds.at[j - 1], dr.at[j - 1], "tp", tp).wait_recv()
+    for half in range(2):
+        for j in order:
+            share_copy(half, j, down(tp, j), tp).wait_recv()
     total = RESIDUAL_SCALE * midf[pl.ds(pl.multiple_of(tp * 8, 8), 8), :]
     for n in range(8):
         total = total + rr[n].astype(F32)
@@ -400,7 +433,7 @@
 ):
     down_rows = jnp.swapaxes(shrink, 0, 1)
     dma = pltpu.SemaphoreType.DMA
-    sems = [(8,)] * 4 + [(2, 4, 2)] * 4 + [(3,), (3,), (1,), (1,), (3,), (3,)] + [(7,)] * 10 + [(6,), (4,), (6,)]
+    sems = [(2, 4)] * 4 + [(2, 4, 3)] * 4 + [(3,), (3,), (1,), (1,), (3,), (3,)] + [(7,)] * 8 + [(2, 7)] * 2 + [(6,), (4,), (6,)]
     return pl.pallas_call(
         body,
         out_shape=jax.ShapeDtypeStruct((8, 2048), BF16),

time: 94.9 us -> 88.4 us (0.932)
  Pallas kernels: 93.3 us -> 86.4 us
    pallas_call x1, Pallas kernels: 93.3 us -> 86.4 us  [shards(): pl.pallas_call(body, out_shape=jax.ShapeDtypeStruct((8, 2048), BF16), in_...]
where the time goes in v3:
time: 88.4 us; the launch traced here: 87.8 us
  Pallas kernels  86.4 us (98%)
  local copies, waits for them, and re-layouts  1.38 us (2%)
    pallas_call x1, Pallas kernels, shards(): pl.pallas_call(body, out_shape=jax.ShapeDtypeStruct((8, 2048), BF16), in_...  86.4 us

profile of v3, /device:TPU:1, one launch (start us, length us, event | category | flops | bytes accessed | tf_op | source)
XLA Modules:
  0.0 87.8 jit_solution(2964046553074984239)
XLA Ops:
  0.0 86.4 %shard_map.154 = bf16[8,2048]{1,0:T(8,128)(2,1)} custom-call(bf16[64,2048]{1,0:T(8,128)(2,1)} %skip_hbm.1, bf16[64,128]{1,0:T(8,128)(2,1)} %q_hbm.1, bf16[64,128]{1,0:T(8,128)(2,1)} %key_hbm.1, bf16[64,128]{1,0:T(8,128)(2,1)} %val_hbm.1, bf16[64,128]{1,0:T(8,128)(2,1)} %valve_hbm.1, bf16[2,64,128]{2,1,0:T(8,128)(2,1)} %fade_hbm.1, ...), custom_call_target="tpu_custom_call" | custom-call | tf_op jit(solution)/shard_map/pallas_call | solution.py:437
  86.4 1.4 %copy.18 = bf16[8,2048]{1,0:T(8,128)(2,1)} copy(bf16[8,2048]{1,0:T(8,128)(2,1)} %shard_map.154) | data formatting | bytes 65536

commit v4 on v3

--- a/solution.py
+++ b/solution.py
@@ -162,16 +162,6 @@
     ones = head_ones()
     spread_heads = jnp.where((iota((2, 128), 1) >> 6) == iota((2, 128), 0), 1.0, 0.0).astype(F32)
     inv = lax.rsqrt(dot(key * key, ones) + KEY_EPS)
-    sides = []
-    for d in range(2):
-        k, passed, written, g_all, vw, qc = local_mixer(
-            q, key, val, inv, fade_ref[d].astype(F32), amend_ref[d].astype(F32),
-            dot(extra_ref[d], spread_heads, 0, 0), d
-        )
-        passed, written = passed.astype(BF16), written.astype(BF16)
-        for part in range(4):
-            c1s[4 * d + part] = jnp.concatenate([passed, written[16 * part : 16 * part + 16]], 0)
-        sides.append((k, g_all, vw, qc))
     for c in weight_copies:
         c.wait()
     wa[z, y] = jnp.concatenate([gate_ref[:, :640], wide_ref[:, :512]], 1)
@@ -179,7 +169,6 @@
     wb[z, y, :, 128:256] = jnp.concatenate([gate_ref[:, 640:], wide_ref[:, 640:]], 1)
     wb[z, y, :, 256:896] = drow_ref[:, :640]
     wb[z, y, :, 896:] = jnp.concatenate([drow_ref[:, 640:], jnp.zeros((32, 64), BF16)], 1)
-    pl.semaphore_wait(barrier, 21)
     def first(k, start):
         for way in range(2):
             back, on = (down, up) if way == 0 else (up, down)
@@ -231,16 +220,30 @@
                 for c in whole(s, p, way):
                     c.wait_recv()
 
-    first(1, True)
-    send(1, 0, (0,))
+    def begin():
+        pl.semaphore_wait(barrier, 21)
+        first(1, True)
+        send(1, 0, (0,))
+        for j in (1, 3, 2):
+            go(copy(pb.at[tp], pb.at[tp], p1s.at[j - 1], p1r.at[j - 1], "tp", 2 * up(xc, j, 4) + core))
+        go(copy(pb.at[tp], pb.at[tp], p2s.at[0], p2r.at[0], "tp", partner))
+
+    sides = []
+    for d in range(2):
+        if d == 1:
+            begin()
+        k, passed, written, g_all, vw, qc = local_mixer(
+            q, key, val, inv, fade_ref[d].astype(F32), amend_ref[d].astype(F32),
+            dot(extra_ref[d], spread_heads, 0, 0), d
+        )
+        passed, written = passed.astype(BF16), written.astype(BF16)
+        for part in range(4):
+            c1s[4 * d + part] = jnp.concatenate([passed, written[16 * part : 16 * part + 16]], 0)
+        sides.append((k, g_all, vw, qc))
     for j in order:
         w = up(y, j)
         go(copy(c1s.at[w], c1r.at[y], x1s.at[j - 1], x1r.at[j - 1], "sp_1", w))
     c1r[y] = c1s[y]
-    for j in (1, 3, 2):
-        go(copy(pb.at[tp], pb.at[tp], p1s.at[j - 1], p1r.at[j - 1], "tp", 2 * up(xc, j, 4) + core))
-    go(copy(pb.at[tp], pb.at[tp], p2s.at[0], p2r.at[0], "tp", partner))
-
     first(1, False)
     first(2, True)
     send(1, 0, (1, 7))

time: 88.4 us -> 86.2 us (0.975)
  Pallas kernels: 86.4 us -> 84.1 us
    pallas_call x1, Pallas kernels: 86.4 us -> 84.1 us  [shards(): pl.pallas_call(body, out_shape=jax.ShapeDtypeStruct((8, 2048), BF16), in_...]
where the time goes in v4:
time: 86.2 us; the launch traced here: 85.4 us
  Pallas kernels  84.1 us (98%)
  local copies, waits for them, and re-layouts  1.38 us (2%)
    pallas_call x1, Pallas kernels, shards(): pl.pallas_call(body, out_shape=jax.ShapeDtypeStruct((8, 2048), BF16), in_...  84.1 us

profile of v4, /device:TPU:1, one launch (start us, length us, event | category | flops | bytes accessed | tf_op | source)
XLA Modules:
  0.0 85.4 jit_solution(3771408086652185763)
XLA Ops:
  0.0 84.1 %shard_map.154 = bf16[8,2048]{1,0:T(8,128)(2,1)} custom-call(bf16[64,2048]{1,0:T(8,128)(2,1)} %skip_hbm.1, bf16[64,128]{1,0:T(8,128)(2,1)} %q_hbm.1, bf16[64,128]{1,0:T(8,128)(2,1)} %key_hbm.1, bf16[64,128]{1,0:T(8,128)(2,1)} %val_hbm.1, bf16[64,128]{1,0:T(8,128)(2,1)} %valve_hbm.1, bf16[2,64,128]{2,1,0:T(8,128)(2,1)} %fade_hbm.1, ...), custom_call_target="tpu_custom_call" | custom-call | tf_op jit(solution)/shard_map/pallas_call | solution.py:440
  84.1 1.4 %copy.18 = bf16[8,2048]{1,0:T(8,128)(2,1)} copy(bf16[8,2048]{1,0:T(8,128)(2,1)} %shard_map.154) | data formatting | bytes 65536

commit v5 on v4

--- a/solution.py
+++ b/solution.py
@@ -103,7 +103,7 @@
     again_ref, mgain_ref, gate_ref, wide_ref, drow_ref, cgain_ref,
     wa, wb, pb, c1s, c1r, c2s, c2r, c3s, c3r, mb, rs, rr, midf, midb, gu,
     a1s, a1r, b1s, b1r, a2s, a2r, b2s, b2r, p1s, p1r, p2s, p2r, p3s, p3r,
-    x1s, x1r, x2s, x2r, x3s, x3r, ms, mr, ds, dr, early, weighty, late,
+    x1s, x1r, x2s, x2r, x3s, x3r, ms, mr, ds, dr, early, weighty, late, relay,
 ):
     z, y, tp = lax.axis_index("sp_0"), lax.axis_index("sp_1"), lax.axis_index("tp")
     xc, core = tp // 2, tp % 2
@@ -122,9 +122,17 @@
         )
 
     barrier = pltpu.get_barrier_semaphore()
-    for axis, at in (("sp_0", z), ("sp_1", y), ("tp", tp)):
-        for j in range(1, 8):
-            pl.semaphore_signal(barrier, inc=1, device_id={axis: up(at, j)}, device_id_type=MESH)
+    near = [("sp_0", up(z, 1)), ("sp_0", down(z, 1)), ("sp_1", up(y, 1)), ("sp_1", down(y, 1))]
+    for axis, at in near + [("tp", up(tp, j)) for j in range(1, 8)]:
+        pl.semaphore_signal(barrier, inc=1, device_id={axis: at}, device_id_type=MESH)
+
+    def pass_word(n):
+        if n > 0:
+            pl.semaphore_wait(relay.at[n - 1], 4)
+        if n < 3:
+            for axis, at in near:
+                pl.semaphore_signal(relay.at[n], inc=1, device_id={axis: at}, device_id_type=MESH)
+
 
     def fetch(pairs, sem):
         copies = [pltpu.make_async_copy(a, b, sem.at[n]) for n, (a, b) in enumerate(pairs)]
@@ -156,18 +164,15 @@
         c.start()
         sent.append(c)
 
-    for c in early_copies:
-        c.wait()
-    q, key, val = q_ref[...].astype(F32), key_ref[...].astype(F32), val_ref[...].astype(F32)
-    ones = head_ones()
-    spread_heads = jnp.where((iota((2, 128), 1) >> 6) == iota((2, 128), 0), 1.0, 0.0).astype(F32)
-    inv = lax.rsqrt(dot(key * key, ones) + KEY_EPS)
     for c in weight_copies:
         c.wait()
-    wa[z, y] = jnp.concatenate([gate_ref[:, :640], wide_ref[:, :512]], 1)
-    wb[z, y, :, :128] = wide_ref[:, 512:640]
-    wb[z, y, :, 128:256] = jnp.concatenate([gate_ref[:, 640:], wide_ref[:, 640:]], 1)
-    wb[z, y, :, 256:896] = drow_ref[:, :640]
+    wa[z, y, :, :384] = gate_ref[:, :384]
+    wa[z, y, :, 384:768] = wide_ref[:, :384]
+    wa[z, y, :, 768:] = drow_ref[:, :384]
+    wb[z, y, :, :256] = gate_ref[:, 384:640]
+    wb[z, y, :, 256:512] = wide_ref[:, 384:640]
+    wb[z, y, :, 512:640] = jnp.concatenate([gate_ref[:, 640:], wide_ref[:, 640:]], 1)
+    wb[z, y, :, 640:896] = drow_ref[:, 384:640]
     wb[z, y, :, 896:] = jnp.concatenate([drow_ref[:, 640:], jnp.zeros((32, 64), BF16)], 1)
     def first(k, start):
         for way in range(2):
@@ -187,51 +192,63 @@
     held = []
 
     def piece(s, p, way):
+        every, ahead, after = (0, WA_COLS, 0, WB_COLS), (0, 768, 0, 640), (768, WA_COLS, 640, WB_COLS)
         if s < 4:
-            return PIECES[p]
-        return (((0, 1, 7), (2,), ()), ((), (6,), (3, 5, 4)))[way][p]
+            return PIECES[p], every
+        if way == 0:
+            return (((0, 1, 7), ahead), ((2,), ahead), ((0, 1, 7, 2), after))[p]
+        return (((6, 3, 5, 4), after), ((6,), ahead), ((3, 5, 4), ahead))[p]
 
     def ring_sems(s, p, way):
         return (a2s.at[way, s - 1, p], a2r.at[way, s - 1, p]), (b2s.at[way, s - 1, p], b2r.at[way, s - 1, p])
 
     def whole(s, p, way):
-        n = len(piece(s, p, way))
+        blocks, (a0, a1, b0, b1) = piece(s, p, way)
         a_sems, b_sems = ring_sems(s, p, way)
-        return (
-            copy(wa.at[0, 0:n], wa.at[0, 0:n], *a_sems, "sp_0", z),
-            copy(wb.at[0, 0:n], wb.at[0, 0:n], *b_sems, "sp_1", y),
-        )
-
-    def send(s, p, only=None):
-        for way in range(2):
+        a, b = wa.at[0, 0 : len(blocks), :, a0:a1], wb.at[0, 0 : len(blocks), :, b0:b1]
+        return copy(a, a, *a_sems, "sp_0", z), copy(b, b, *b_sems, "sp_1", y)
+
+    def send(s, p, only=None, ways=(0, 1)):
+        for way in ways:
             back, on = (down, up) if way == 0 else (up, down)
+            blocks, (a0, a1, b0, b1) = piece(s, p, way)
             a_sems, b_sems = ring_sems(s, p, way)
             n, m = back(z, s - 1), back(y, s - 1)
-            for e in piece(s, p, way) if only is None else only:
-                a, b = wa.at[n, up(y, e)], wb.at[up(z, e), m]
+            for e in blocks if only is None else only:
+                a, b = wa.at[n, up(y, e), :, a0:a1], wb.at[up(z, e), m, :, b0:b1]
                 copy(a, a, *a_sems, "sp_0", on(z, 1)).start()
                 copy(b, b, *b_sems, "sp_1", on(y, 1)).start()
-            if piece(s, p, way) and (only is None or only[-1] == PIECES[p][-1]):
+            if only is None or only[-1] == blocks[-1]:
                 held.extend(whole(s, p, way))
 
-    def take(s, p):
-        for way in range(2):
-            if piece(s, p, way):
-                for c in whole(s, p, way):
-                    c.wait_recv()
+    def take(s, p, ways=(0, 1)):
+        for way in ways:
+            for c in whole(s, p, way):
+                c.wait_recv()
 
     def begin():
-        pl.semaphore_wait(barrier, 21)
+        pl.semaphore_wait(barrier, 11)
+        pass_word(0)
         first(1, True)
         send(1, 0, (0,))
         for j in (1, 3, 2):
             go(copy(pb.at[tp], pb.at[tp], p1s.at[j - 1], p1r.at[j - 1], "tp", 2 * up(xc, j, 4) + core))
         go(copy(pb.at[tp], pb.at[tp], p2s.at[0], p2r.at[0], "tp", partner))
 
+    begin()
+    for c in early_copies:
+        c.wait()
+    q, key, val = q_ref[...].astype(F32), key_ref[...].astype(F32), val_ref[...].astype(F32)
+    ones = head_ones()
+    spread_heads = jnp.where((iota((2, 128), 1) >> 6) == iota((2, 128), 0), 1.0, 0.0).astype(F32)
+    inv = lax.rsqrt(dot(key * key, ones) + KEY_EPS)
     sides = []
     for d in range(2):
+        pass_word(d + 1)
         if d == 1:
-            begin()
+            first(1, False)
+            first(2, True)
+            send(1, 0, (1, 7))
         k, passed, written, g_all, vw, qc = local_mixer(
             q, key, val, inv, fade_ref[d].astype(F32), amend_ref[d].astype(F32),
             dot(extra_ref[d], spread_heads, 0, 0), d
@@ -240,13 +257,11 @@
         for part in range(4):
             c1s[4 * d + part] = jnp.concatenate([passed, written[16 * part : 16 * part + 16]], 0)
         sides.append((k, g_all, vw, qc))
+    pass_word(3)
     for j in order:
         w = up(y, j)
         go(copy(c1s.at[w], c1r.at[y], x1s.at[j - 1], x1r.at[j - 1], "sp_1", w))
     c1r[y] = c1s[y]
-    first(1, False)
-    first(2, True)
-    send(1, 0, (1, 7))
 
     for c in late_copies:
         c.wait()
@@ -366,17 +381,19 @@
     midb[...] = midf[...].astype(BF16)
 
     take(3, 0)
-    send(4, 0)
+    send(4, 0, None, (0,))
     take(3, 1)
     send(4, 1)
+    send(4, 2, None, (0,))
     take(3, 2)
-    send(4, 2)
+    send(4, 2, None, (1,))
+    send(4, 0, None, (1,))
 
     gu[...] = jnp.zeros_like(gu)
 
     def widen(n):
         mid = midb[:, pl.ds(pl.multiple_of(n * 256, 256), 256)]
-        gu[:, :1152] += bdot(mid, wa[n].reshape(256, 1152))
+        gu[:, :768] += bdot(mid, wa[n, :, :, :768].reshape(256, 768))
 
     def widen_near(n, carry):
         widen(up(z, n + 5))
@@ -384,42 +401,47 @@
 
     def widen_rest(n, carry):
         mid = midb[:, pl.ds(pl.multiple_of(n * 256, 256), 256)]
-        gu[:, 1152:] += bdot(mid, wb[n, :, :, :256].reshape(256, 256))
+        gu[:, 768:] += bdot(mid, wb[n, :, :, :640].reshape(256, 640))
         return carry
 
     lax.fori_loop(0, 7, widen_near, 0)
-    take(4, 0)
+    take(4, 0, (0,))
     take(4, 1)
-    take(4, 2)
+    take(4, 2, (1,))
     widen(up(z, 4))
     lax.fori_loop(0, 8, widen_rest, 0)
 
-    gate, wide = gu[:, :640], gu[:, 640:1280]
-    tail = gu[:, 1280:]
+    gate, wide = gu[:, :384], gu[:, 384:768]
+    gate_b, wide_b, tail = gu[:, 768:1024], gu[:, 1024:1280], gu[:, 1280:]
     main = gate / (1.0 + jnp.exp(-gate)) * wide
+    main_b = gate_b / (1.0 + jnp.exp(-gate_b)) * wide_b
     rest = tail / (1.0 + jnp.exp(-tail)) * pltpu.roll(tail, 64, 1)
     rest = jnp.where(iota((64, 128), 1) < 64, rest, 0.0)
-    inner = jnp.concatenate([main, rest], 1).astype(BF16)
+    inner = main.astype(BF16)
+    inner_b = jnp.concatenate([main_b, rest], 1).astype(BF16)
+    take(4, 2, (0,))
+    take(4, 0, (1,))
 
     def shrink(n, carry):
         cols = pl.ds(pl.multiple_of(n * 256, 256), 256)
-        share = bdot(inner, wb[n, :, :, 256:].reshape(256, 768), 1, 1)
+        share = bdot(inner, wa[n, :, :, 768:].reshape(256, 384), 1, 1)
+        share += bdot(inner_b, wb[n, :, :, 640:].reshape(256, 384), 1, 1)
         for m in range(8):
             rs[m, :, cols] = share[8 * m : 8 * m + 8].astype(BF16)
         return carry
 
     def share_copy(half, j, source, target):
-        cols = slice(1024 * half, 1024 * half + 1024)
+        cols = slice(512 * half, 512 * half + 512)
         return copy(
             rs.at[target, :, cols], rr.at[source, :, cols], ds.at[half, j - 1], dr.at[half, j - 1], "tp", target
         )
 
-    for half in range(2):
-        lax.fori_loop(4 * half, 4 * half + 4, shrink, 0)
+    for half in range(4):
+        lax.fori_loop(2 * half, 2 * half + 2, shrink, 0)
         for j in order:
             go(share_copy(half, j, tp, up(tp, j)))
     rr[tp] = rs[tp]
-    for half in range(2):
+    for half in range(4):
         for j in order:
             share_copy(half, j, down(tp, j), tp).wait_recv()
     total = RESIDUAL_SCALE * midf[pl.ds(pl.multiple_of(tp * 8, 8), 8), :]
@@ -436,7 +458,7 @@
 ):
     down_rows = jnp.swapaxes(shrink, 0, 1)
     dma = pltpu.SemaphoreType.DMA
-    sems = [(2, 4)] * 4 + [(2, 4, 3)] * 4 + [(3,), (3,), (1,), (1,), (3,), (3,)] + [(7,)] * 8 + [(2, 7)] * 2 + [(6,), (4,), (6,)]
+    sems = [(2, 4)] * 4 + [(2, 4, 3)] * 4 + [(3,), (3,), (1,), (1,), (3,), (3,)] + [(7,)] * 8 + [(4, 7)] * 2 + [(6,), (4,), (6,)]
     return pl.pallas_call(
         body,
         out_shape=jax.ShapeDtypeStruct((8, 2048), BF16),
@@ -474,7 +496,8 @@
             pltpu.VMEM((64, 2048), BF16),
             pltpu.VMEM((64, 1408), F32),
         ]
-        + [dma(s) for s in sems],
+        + [dma(s) for s in sems]
+        + [pltpu.SemaphoreType.REGULAR((3,))],
         compiler_params=pltpu.CompilerParams(
             collective_id=0, has_side_effects=True, vmem_limit_bytes=67043328
         ),

time: 86.2 us -> 85 us (0.986)
  no operation moved by 1% of the time
where the time goes in v5:
time: 85 us; the launch traced here: 84.8 us
  Pallas kernels  83.4 us (98%)
  local copies, waits for them, and re-layouts  1.38 us (2%)
    pallas_call x1, Pallas kernels, shards(): pl.pallas_call(body, out_shape=jax.ShapeDtypeStruct((8, 2048), BF16), in_...  83.4 us

profile of v5, /device:TPU:1, one launch (start us, length us, event | category | flops | bytes accessed | tf_op | source)
XLA Modules:
  0.0 84.8 jit_solution(18022310600249431656)
XLA Ops:
  0.0 83.4 %shard_map.154 = bf16[8,2048]{1,0:T(8,128)(2,1)} custom-call(bf16[64,2048]{1,0:T(8,128)(2,1)} %skip_hbm.1, bf16[64,128]{1,0:T(8,128)(2,1)} %q_hbm.1, bf16[64,128]{1,0:T(8,128)(2,1)} %key_hbm.1, bf16[64,128]{1,0:T(8,128)(2,1)} %val_hbm.1, bf16[64,128]{1,0:T(8,128)(2,1)} %valve_hbm.1, bf16[2,64,128]{2,1,0:T(8,128)(2,1)} %fade_hbm.1, ...), custom_call_target="tpu_custom_call" | custom-call | tf_op jit(solution)/shard_map/pallas_call | solution.py:462
  83.4 1.4 %copy.18 = bf16[8,2048]{1,0:T(8,128)(2,1)} copy(bf16[8,2048]{1,0:T(8,128)(2,1)} %shard_map.154) | data formatting | bytes 65536
